TPU v7x, 128 devices: a whole 4x4x4 slice. The times are simulated.
128 devices in a mesh: sp: 64 (over z, y, x), tp: 2 (over core).
Axes of the slice: x: 4, y: 4, z: 4, core: 2. Of those that a mesh axis runs over, the one named last changes fastest.
Arguments:
- conv_value: bfloat16 [16384, 1024], P('sp', 'tp'), may hold values from -6 to 6
- conv_gate: bfloat16 [16384, 1024], P('sp', 'tp'), may hold values from -6 to 6
- taps: bfloat16 [31, 1024], P(None, 'tp'), may hold values from -1 to 1
- doc_ids: int32 [16384], P('sp'), may hold values from 0 to 15, never falling along the last dimension, each value on 1 to 2048 neighbouring positions
- gn_gain: float32 [1024], P('tp'), may hold values from 0.1 to 1.9
- gn_shift: float32 [1024], P('tp'), may hold values from -3 to 3
- conv_out: bfloat16 [1024, 2048], replicated, may hold values from -0.1875 to 0.1875
- residual: bfloat16 [16384, 2048], P(('sp', 'tp')), may hold values from -6 to 6
- norm_gain: float32 [2048], replicated, may hold values from 0.1 to 1.9
- routes: int32 [16384, 2], P(('sp', 'tp')), may hold values from 0 to 127, as said below
- route_weight: float32 [16384, 2], P(('sp', 'tp')), may hold values from 0.3 to 1.2
- expert_gate: bfloat16 [128, 2048, 512], P(('sp', 'tp')), may hold values from -0.125 to 0.125
- expert_up: bfloat16 [128, 2048, 512], P(('sp', 'tp')), may hold values from -0.125 to 0.125
- expert_down: bfloat16 [128, 512, 2048], P(('sp', 'tp')), may hold values from -0.25 to 0.25
- shared_gate: bfloat16 [2048, 512], replicated, may hold values from -0.125 to 0.125
- shared_up: bfloat16 [2048, 512], replicated, may hold values from -0.125 to 0.125
- shared_down: bfloat16 [512, 2048], replicated, may hold values from -0.25 to 0.25
Outputs:
- layer_out: bfloat16 [16384, 2048], P(('sp', 'tp'))
Inputs may be any that keep to these rules, and one draw needn't show every extreme that they name: `routes`: each row names 2 different experts. The rows of one device name each expert at most 4 times, and one expert, the same for every device, exactly 4 times. `doc_ids`: numbers never fall from one position to the next.
All inputs are finite; a program needn't handle non-finite values.
Results may differ from a plain program's by a relative error of at most 0.014.
Values may be sent and summed in bfloat16 or wider, within the bound.
No kernel may reach another device: no remote copies, remote signals or barrier semaphores. Data moves between devices by JAX's collectives and lax.ppermute only.
A program may use at most 128 MiB of HBM per device.

v0:
```python
import jax
import jax.numpy as jnp
from jax import lax
from jax.sharding import PartitionSpec as P

GROUPS = 8


epsilon = 1e-06


def from_behind(x, axis, by):
    peers = lax.axis_size(axis)
    pairs = [(i, i + by) for i in range(peers) if 0 <= i + by < peers]
    return lax.ppermute(x, axis, pairs)


def per_device(
    conv_value,
    conv_gate,
    taps,
    doc_ids,
    gn_gain,
    gn_shift,
    conv_out,
    residual,
    norm_gain,
    routes,
    route_weight,
    expert_gate,
    expert_up,
    expert_down,
    shared_gate,
    shared_up,
    shared_down,
):
    position_count, channel_count = conv_value.shape
    kernel_width = taps.shape[0]
    model_width = residual.shape[1]
    glu_out = (
        conv_value.astype(jnp.float32) * jax.nn.sigmoid(conv_gate.astype(jnp.float32))
    ).astype(jnp.bfloat16)
    rim_start = position_count - kernel_width + 1
    edge_glu, edge_ids = from_behind((glu_out[rim_start:], doc_ids[rim_start:]), "sp", 1)
    longer_glu = jnp.concatenate([edge_glu, glu_out], axis=0)
    longer_ids = jnp.concatenate([edge_ids, doc_ids], axis=0)
    conv_sum = jnp.zeros((position_count, channel_count), jnp.float32)
    for offset in range(kernel_width):
        same_doc = (longer_ids[offset : offset + position_count] == doc_ids)[:, None]
        tap_term = taps[offset].astype(jnp.float32)[None, :] * longer_glu[
            offset : offset + position_count
        ].astype(jnp.float32)
        conv_sum = conv_sum + jnp.where(same_doc, tap_term, 0.0)
    core_split = lax.axis_size("tp")
    groups_here = GROUPS // core_split
    grouped = conv_sum.reshape(position_count, groups_here, channel_count // groups_here)
    group_mean = jnp.mean(grouped, axis=-1, keepdims=True)
    centered = grouped - group_mean
    group_var = jnp.mean(centered * centered, axis=-1, keepdims=True)
    normalized = (centered * lax.rsqrt(group_var + epsilon)).reshape(position_count, channel_count)
    conv_act = jax.nn.silu(normalized * gn_gain + gn_shift).astype(jnp.bfloat16)
    token_rows = lax.all_to_all(conv_act, "tp", split_axis=0, concat_axis=1, tiled=True)
    projected = jnp.dot(token_rows, conv_out, preferred_element_type=jnp.float32)
    stream = (residual.astype(jnp.float32) + projected).astype(jnp.bfloat16)
    stream_wide = stream.astype(jnp.float32)
    normed = (
        stream_wide
        * lax.rsqrt(jnp.mean(stream_wide * stream_wide, axis=-1, keepdims=True) + epsilon)
        * norm_gain
    ).astype(jnp.bfloat16)
    token_count, top_count = routes.shape
    sequence_split = lax.axis_size("sp")
    device_count = sequence_split * core_split
    local_experts = expert_gate.shape[0]
    experts = local_experts * device_count
    capacity = 2 * token_count * top_count // experts
    flat_routes = routes.reshape(-1)
    onehot = (flat_routes[:, None] == jnp.arange(experts, dtype=jnp.int32)[None, :]).astype(
        jnp.int32
    )
    slot_index = jnp.sum(jnp.cumsum(onehot, axis=0) * onehot, axis=1) - 1
    target = flat_routes * capacity + slot_index
    source = (
        jnp.full((experts * capacity,), token_count, jnp.int32)
        .at[target]
        .set(jnp.arange(token_count * top_count, dtype=jnp.int32) // top_count)
    )
    padded_rows = jnp.concatenate([normed, jnp.zeros((1, model_width), normed.dtype)], axis=0)
    outgoing = padded_rows[source]
    shared_hidden = (
        jax.nn.silu(jnp.dot(normed, shared_gate, preferred_element_type=jnp.float32))
        * jnp.dot(normed, shared_up, preferred_element_type=jnp.float32)
    ).astype(jnp.bfloat16)
    shared_out = jnp.dot(shared_hidden, shared_down, preferred_element_type=jnp.float32)
    parcel = outgoing.reshape(device_count, local_experts, capacity, model_width)
    arrived = lax.all_to_all(parcel, ("sp", "tp"), split_axis=0, concat_axis=0, tiled=True)
    expert_rows = arrived[:, 0].reshape(-1, model_width)
    gate_part = jnp.dot(expert_rows, expert_gate[0], preferred_element_type=jnp.float32)
    up_part = jnp.dot(expert_rows, expert_up[0], preferred_element_type=jnp.float32)
    hidden = (jax.nn.silu(gate_part) * up_part).astype(jnp.bfloat16)
    result = jnp.dot(hidden, expert_down[0], preferred_element_type=jnp.float32).astype(
        jnp.bfloat16
    )
    results = [result.reshape(arrived.shape[0], arrived.shape[2], model_width)]
    returned = lax.all_to_all(
        jnp.stack(results, axis=1), ("sp", "tp"), split_axis=0, concat_axis=0, tiled=True
    )
    picked = returned.reshape(experts * capacity, model_width)[target].reshape(
        token_count, top_count, model_width
    )
    routed = jnp.zeros((token_count, model_width), jnp.float32)
    for route_index in range(top_count):
        routed = routed + route_weight[:, route_index, None] * picked[:, route_index].astype(
            jnp.float32
        )
    return (stream_wide + shared_out + routed).astype(jnp.bfloat16)


def solution(mesh):
    return jax.shard_map(
        per_device,
        mesh=mesh,
        in_specs=(
            P("sp", "tp"),
            P("sp", "tp"),
            P(None, "tp"),
            P("sp"),
            P("tp"),
            P("tp"),
            P(),
            P(("sp", "tp"), None),
            P(),
            P(("sp", "tp"), None),
            P(("sp", "tp"), None),
            P(("sp", "tp"), None, None),
            P(("sp", "tp"), None, None),
            P(("sp", "tp"), None, None),
            P(),
            P(),
            P(),
        ),
        out_specs=P(("sp", "tp"), None),
        check_vma=False,
    )
```

profile of v0, /device:TPU:1, one launch (start us, length us, event | category | flops | bytes accessed | tf_op | source)
XLA Modules:
  0.0 152.2 jit_solution(11476483469996541821)
XLA Ops:
  0.0 0.0 copy-start
  0.0 0.0 copy-start.4
  0.0 0.9 slice.297
  0.9 3.9 %collective-permute-start = (s32[30]{0:T(128)S(1)}, s32[30]{0:T(128)S(1)}, u32[]{:S(2)}, u32[]{:S(2)}) collective-permute-start(s32[30]{0:T(128)S(1)} %slice.297), channel_id=1, source_target_pairs={{0,2},{2,4},{4,6},{6,8},{8,10},{10,12},{12,14},{14,16},{16,18},{18... | collective-permute-start | bytes 368 | tf_op jit(solution)/shard_map/ppermute | solution.py:15
  4.8 1.2 multiply_convert_fusion.2
  6.1 3.1 %collective-permute-start.1 = (bf16[30,512]{1,0:T(8,128)(2,1)S(1)}, bf16[30,512]{1,0:T(8,128)(2,1)S(1)}, u32[]{:S(2)}, u32[]{:S(2)}) collective-permute-start(bf16[30,512]{1,0:T(8,128)(2,1)S(1)} %slice.400), channel_id=1, source_target_pairs={{0,2},{2,4},{4,6},{6,8},{8,10},{10,12},{12,14},{14,16},{16,18},{18... | collective-permute-start | bytes 92168 | tf_op jit(solution)/shard_map/ppermute | solution.py:15
  9.2 1.0 slice_convert_fusion.30
  10.2 1.0 slice_convert_fusion.29
  11.2 0.8 copy.35
  12.0 0.1 eq.149
  12.1 0.1 eq.145
  12.3 0.7 broadcast_multiply_fusion.1
  13.0 0.1 copy.37
  13.1 0.2 fusion.56
  13.4 0.2 fusion.57
  13.6 0.1 copy.34
  13.7 0.1 mul.647
  13.8 1.4 scatter_custom_fusion
  15.3 0.0 collective-permute-done
  15.3 0.0 copy-done.4
  15.3 0.1 pad_add_fusion
  15.4 0.1 slice_compare_fusion.29
  15.5 0.1 slice_compare_fusion.28
  15.6 0.0 collective-permute-done.1
  15.6 4.0 %multiply_add_fusion = f32[256,512]{1,0:T(8,128)S(1)} fusion(bf16[256,512]{1,0:T(8,128)(2,1)S(1)} %multiply_convert_fusion.2, bf16[30,512]{1,0:T(8,128)(2,1)S(1)} %collective-permute-done.1, f32[512]{0:T(512)S(1)} %bitcast.142, f32[512]{0:T(512)S(1)} %bitcast.143, f32[512]{0:T(512)S(1)} %bitcast.114, f32[512]{0:T(512)S(1)} %bitcast.115, ...), kind=kLoop, calls=%fused_computation.62 | loop fusion | flops 27787264 | bytes 888320 | tf_op jit(solution)/shard_map/add | solution.py:53
  19.6 0.0 copy-start.6
  19.6 0.0 copy-start.7
  19.6 0.2 reshape.126
  19.8 0.3 reduce_sum.36
  20.2 0.6 multiply_reduce_fusion.1
  20.9 0.0 copy-start.3
  20.9 0.3 mul.630
  21.2 0.3 sub.25
  21.5 0.0 copy-done.6
  21.6 0.0 copy-done.7
  21.6 0.2 multiply_convert_fusion.1
  21.8 4.8 %all_to_all.29 = bf16[2,128,512]{2,1,0:T(8,128)(2,1)S(1)} all-to-all(bf16[2,128,512]{2,1,0:T(8,128)(2,1)S(1)} %bitcast.107), channel_id=1, replica_groups=mesh['sp'=64,'tp'=2] {'tp'}, dimensions={0} | all-to-all | bytes 524288 | tf_op jit(solution)/shard_map/all_to_all | solution.py:62
  26.6 0.2 copy.33
  26.8 0.0 copy-done.3
  26.8 0.0 copy-start.5
  26.8 3.0 %multiply_reduce_fusion = (f32[128]{0:T(128)S(1)}, f32[128,2048]{1,0:T(8,128)S(1)}) fusion(bf16[128,1024]{0,1:T(8,128)(2,1)S(1)} %bitcast.108, bf16[1024,2048]{1,0:T(8,128)(2,1)} %param.23, bf16[128,2048]{1,0:T(8,128)(2,1)S(1)} %copy-done.3), kind=kOutput, calls=%fused_computation.52 | convolution fusion | flops 538443648 | bytes 6029824 | tf_op jit(solution)/shard_map/dot_general | solution.py:63
  29.8 0.0 copy-start.2
  29.8 1.0 copy-done.2
  30.8 0.0 copy-done.5
  30.8 0.2 multiply_convert_fusion
  31.0 0.0 copy-start.1
  31.0 3.3 %gather_fusion = bf16[512,2048]{1,0:T(8,128)(2,1)} fusion(bf16[129,2048]{1,0:T(8,128)(2,1)S(1)} %concatenate.11, s32[1024]{0:T(1024)S(1)} %pad_clamp_fusion.1), kind=kCustom, calls=%fused_computation | custom fusion | bytes 4196352 | tf_op jit(solution)/shard_map/gather | solution.py:89
  34.3 4.1 %reshape.128 = bf16[128,1,4,2048]{3,2,0,1:T(4,128)(2,1)} reshape(bf16[512,2048]{1,0:T(8,128)(2,1)} %gather_fusion) | data formatting | bytes 4194304 | tf_op jit(solution)/shard_map/reshape | solution.py:95
  38.4 40.4 %all_to_all.30 = bf16[128,1,4,2048]{3,2,1,0:T(4,128)(2,1)} all-to-all(bf16[128,1,4,2048]{3,2,1,0:T(4,128)(2,1)} %bitcast.104), channel_id=1, replica_groups=mesh['sp'=64,'tp'=2] {'sp','tp'}, dimensions={0} | all-to-all | bytes 4194304 | tf_op jit(solution)/shard_map/all_to_all | solution.py:96
  78.8 3.9 %reshape_squeeze.3 = bf16[512,2048]{1,0:T(8,128)(2,1)} reshape(bf16[128,1,4,2048]{3,2,1,0:T(4,128)(2,1)} %all_to_all.30) | data formatting | bytes 4194304 | tf_op jit(solution)/shard_map/reshape;squeeze | solution.py:97
  82.8 4.4 %fusion.7 = f32[512,512]{1,0:T(8,128)} fusion(bf16[512,2048]{1,0:T(8,128)(2,1)} %reshape_squeeze.3, bf16[1,2048,512]{2,1,0:T(8,128)(2,1)} %param.28), kind=kOutput, calls=%fused_computation.42 | convolution fusion | flops 1073741824 | bytes 5242880 | tf_op jit(solution)/shard_map/dot_general | solution.py:98
  87.2 0.0 copy-done
  87.2 6.2 %convolution_convert_fusion = bf16[512,2048]{1,0:T(8,128)(2,1)} fusion(bf16[1,512,2048]{2,1,0:T(8,128)(2,1)S(1)} %copy-done, bf16[512,2048]{1,0:T(8,128)(2,1)} %reshape_squeeze.3, bf16[1,2048,512]{2,1,0:T(8,128)(2,1)} %param.29, f32[512,512]{1,0:T(8,128)} %fusion.7), kind=kOutput, calls=%fused_computation.3 | convolution fusion | flops 2150105088 | bytes 9437184 | tf_op jit(solution)/shard_map/dot_general | solution.py:101
  93.4 4.1 %stack_reshape.3 = bf16[128,1,4,2048]{3,2,0,1:T(4,128)(2,1)} reshape(bf16[512,2048]{1,0:T(8,128)(2,1)} %convolution_convert_fusion) | data formatting | bytes 4194304 | tf_op jit(solution)/shard_map/stack;reshape | solution.py:106
  97.5 5.6 %all-to-all-start.2 = ((bf16[128,1,4,2048]{3,2,1,0:T(4,128)(2,1)}), bf16[128,1,4,2048]{3,2,1,0:T(4,128)(2,1)}, u32[]{:S(2)}, u32[]{:S(2)}) async-start(bf16[128,1,4,2048]{3,2,1,0:T(4,128)(2,1)} %bitcast.103), calls=%async_computation.2 | async-start | bytes 4194304 | tf_op jit(solution)/shard_map/all_to_all | solution.py:105
  103.2 0.0 copy-done.8
  103.2 0.0 copy-done.1
  103.2 2.0 %fusion.66 = f32[128,512]{1,0:T(8,128)S(1)} fusion(bf16[128,2048]{1,0:T(8,128)(2,1)S(1)} %multiply_convert_fusion, bf16[2048,512]{1,0:T(8,128)(2,1)} %param.31), kind=kOutput, calls=%fused_computation.199 | convolution fusion | flops 268435456 | bytes 2883584 | tf_op jit(solution)/shard_map/dot_general | solution.py:91
  105.2 28.2 %all-to-all-done.2 = bf16[128,1,4,2048]{3,2,1,0:T(4,128)(2,1)} async-done(((bf16[128,1,4,2048]{3,2,1,0:T(4,128)(2,1)}), bf16[128,1,4,2048]{3,2,1,0:T(4,128)(2,1)}, u32[]{:S(2)}, u32[]{:S(2)}) %all-to-all-start.2) | async-done | bytes 2097184 | tf_op jit(solution)/shard_map/all_to_all | solution.py:105
  133.4 4.0 %reshape.129 = bf16[512,2048]{1,0:T(8,128)(2,1)} reshape(bf16[128,1,4,2048]{3,2,1,0:T(4,128)(2,1)} %all-to-all-done.2) | data formatting | bytes 4194304 | tf_op jit(solution)/shard_map/reshape | solution.py:108
  137.4 5.2 %gather_fusion.1 = bf16[256,2048]{1,0:T(8,128)(2,1)} fusion(bf16[512,2048]{1,0:T(8,128)(2,1)} %reshape.129, s32[1024]{0:T(1024)S(1)} %pad_clamp_fusion), kind=kCustom, calls=%fused_computation.1 | custom fusion | bytes 2098176 | tf_op jit(solution)/shard_map/gather | solution.py:108
  142.6 1.7 %reshape.130 = bf16[128,2,2048]{2,1,0:T(2,128)(2,1)S(1)} reshape(bf16[256,2048]{1,0:T(8,128)(2,1)} %gather_fusion.1) | data formatting | bytes 2097152 | tf_op jit(solution)/shard_map/reshape | solution.py:108
  144.3 2.5 %fusion.65 = (bf16[128,1,2048]{2,1,0:T(2,128)(2,1)}, bf16[128,1,2048]{2,1,0:T(2,128)(2,1)}) fusion(bf16[128,2,2048]{2,1,0:T(2,128)(2,1)S(1)} %reshape.130), kind=kLoop, calls=%fused_computation.198 | loop fusion | bytes 2097152 | tf_op jit(solution)/shard_map/slice | solution.py:113
  146.8 5.4 %fusion.3 = bf16[128,2048]{1,0:T(8,128)(2,1)} fusion(f32[128,2048]{1,0:T(8,128)} %copy-done.2, bf16[512,2048]{1,0:T(8,128)(2,1)} %param.33, bf16[128,2048]{1,0:T(8,128)(2,1)} %copy-done.1, bf16[2048,512]{1,0:T(8,128)(2,1)} %param.32, bf16[128,1,2048]{2,1,0:T(2,128)(2,1)} %get-tuple-element.6, bf16[128,1,2048]{2,1,0:T(2,128)(2,1)} %get-tuple-element.5, ...), kind=kOutput, calls=%fused_computation.38 | convolution fusion | flops 539361280 | bytes 7603200 | tf_op jit(solution)/shard_map/dot_general | solution.py:94
  (19 shorter events, 0.2 us)
Async XLA Ops:
  0.0 87.2 %copy-start = (bf16[1,512,2048]{2,1,0:T(8,128)(2,1)S(1)}, bf16[1,512,2048]{2,1,0:T(8,128)(2,1)}, u32[]{:S(2)}) copy-start(bf16[1,512,2048]{2,1,0:T(8,128)(2,1)} %param.30) | copy-start | bytes 6291460
  0.0 15.3 %copy-start.4 = (s32[256]{0:T(256)S(1)}, s32[256]{0:T(256)}, u32[]{:S(2)}) copy-start(s32[256]{0:T(256)} %param.20) | copy-start | bytes 3076
  0.9 14.4 %collective-permute-start = (s32[30]{0:T(128)S(1)}, s32[30]{0:T(128)S(1)}, u32[]{:S(2)}, u32[]{:S(2)}) collective-permute-start(s32[30]{0:T(128)S(1)} %slice.297), channel_id=1, source_target_pairs={{0,2},{2,4},{4,6},{6,8},{8,10},{10,12},{12,14},{14,16},{16,18},{18... | collective-permute-start | bytes 368 | tf_op jit(solution)/shard_map/ppermute | solution.py:15
  6.1 9.5 %collective-permute-start.1 = (bf16[30,512]{1,0:T(8,128)(2,1)S(1)}, bf16[30,512]{1,0:T(8,128)(2,1)S(1)}, u32[]{:S(2)}, u32[]{:S(2)}) collective-permute-start(bf16[30,512]{1,0:T(8,128)(2,1)S(1)} %slice.400), channel_id=1, source_target_pairs={{0,2},{2,4},{4,6},{6,8},{8,10},{10,12},{12,14},{14,16},{16,18},{18... | collective-permute-start | bytes 92168 | tf_op jit(solution)/shard_map/ppermute | solution.py:15
  19.6 1.9 %copy-start.6 = (f32[512]{0:T(512)S(1)}, f32[512]{0:T(512)}, u32[]{:S(2)}) copy-start(f32[512]{0:T(512)} %param.22) | copy-start | bytes 6148
  19.6 1.9 %copy-start.7 = (f32[512]{0:T(512)S(1)}, f32[512]{0:T(512)}, u32[]{:S(2)}) copy-start(f32[512]{0:T(512)} %param.21) | copy-start | bytes 6148
  20.9 5.9 %copy-start.3 = (bf16[128,2048]{1,0:T(8,128)(2,1)S(1)}, bf16[128,2048]{1,0:T(8,128)(2,1)}, u32[]{:S(2)}) copy-start(bf16[128,2048]{1,0:T(8,128)(2,1)} %param.24) | copy-start | bytes 1572868
  26.8 4.0 %copy-start.5 = (f32[2048]{0:T(1024)S(1)}, f32[2048]{0:T(1024)}, u32[]{:S(2)}) copy-start(f32[2048]{0:T(1024)} %param.25) | copy-start | bytes 24580
  29.8 1.0 copy-start.2
  31.0 72.2 %copy-start.1 = (bf16[128,2048]{1,0:T(8,128)(2,1)}, bf16[128,2048]{1,0:T(8,128)(2,1)S(1)}, u32[]{:S(2)}) copy-start(bf16[128,2048]{1,0:T(8,128)(2,1)S(1)} %multiply_convert_fusion) | copy-start | bytes 1572868
  97.5 5.6 %copy-start.8 = (f32[128,2]{0,1:T(2,128)S(1)}, f32[128,2]{0,1:T(2,128)}, u32[]{:S(2)}) copy-start(f32[128,2]{0,1:T(2,128)} %param.27) | copy-start | bytes 3076
  97.5 35.9 %all-to-all-start.2 = ((bf16[128,1,4,2048]{3,2,1,0:T(4,128)(2,1)}), bf16[128,1,4,2048]{3,2,1,0:T(4,128)(2,1)}, u32[]{:S(2)}, u32[]{:S(2)}) async-start(bf16[128,1,4,2048]{3,2,1,0:T(4,128)(2,1)} %bitcast.103), calls=%async_computation.2 | async-start | bytes 4194304 | tf_op jit(solution)/shard_map/all_to_all | solution.py:105
where the time goes:
time: 153 us; the launch traced here: 152 us
  blocking collectives  45.2 us (30%)
  local copies, waits for them, and re-layouts  34.7 us (23%)
  waiting for transfers between devices  28.2 us (18%)
  matrix products  21.1 us (14%)
  starting transfers between devices  12.6 us (8%)
  other arithmetic  10 us (7%)
    all_to_all x1, blocking collectives, per_device(): lax.all_to_all(parcel, ('sp', 'tp'), split_axis=0, concat_axis=0, tiled=T...  40.4 us
    all_to_all x1, waiting for transfers between devices, per_device(): lax.all_to_all(jnp.stack(results, axis=1), ('sp', 'tp'), split_axis=0, co...  28.2 us
    ppermute x2, starting transfers between devices, from_behind(): return lax.ppermute(x, axis, pairs)  7.04 us
    dot_general x1, matrix products, per_device(): jnp.dot(hidden, expert_down[0], preferred_element_type=jnp.float32)  6.22 us
    reshape x2, local copies, waits for them, and re-layouts, per_device(): returned.reshape(experts * capacity, model_width)[target]  5.71 us
    all_to_all x1, starting transfers between devices, per_device(): lax.all_to_all(jnp.stack(results, axis=1), ('sp', 'tp'), split_axis=0, co...  5.61 us
    dot_general x1, matrix products, per_device(): jnp.dot(shared_hidden, shared_down, preferred_element_type=jnp.float32)  5.42 us
    gather x1, local copies, waits for them, and re-layouts, per_device(): returned.reshape(experts * capacity, model_width)[target]  5.21 us
  transfers between devices with their start and end apart: 3, of which 1 were waited for; matrix products, arithmetic and copies ran while one was open for 6% of the time, Pallas kernels for 0%

commit v1 on v0

v1 whole, which is shorter than its diff:
```python
import functools

import jax
import jax.numpy as jnp
from jax import lax
from jax.experimental import pallas as pl
from jax.experimental.pallas import tpu as pltpu
from jax.sharding import PartitionSpec as P

GROUPS = 8
EPS = 1e-06
F32 = jnp.float32
BF16 = jnp.bfloat16
HALO = 32
PACK = 40


def from_behind(x, axis, by):
    peers = lax.axis_size(axis)
    pairs = [(i, i + by) for i in range(peers) if 0 <= i + by < peers]
    return lax.ppermute(x, axis, pairs)


def glu_of(value, gate):
    wide = value.astype(F32) * jax.nn.sigmoid(gate.astype(F32))
    return wide.astype(BF16)


def pack_kernel(value, gate, ids, out):
    channels = value.shape[1]
    positions = ids.shape[1]
    out[0:HALO, :] = glu_of(value[...], gate[...])
    tail = ids[:, positions - 128 :].astype(F32)
    row = jnp.concatenate([tail, jnp.zeros((1, channels - 128), F32)], axis=1)
    out[HALO:, :] = jnp.broadcast_to(row, (PACK - HALO, channels)).astype(BF16)


def conv_kernel(value, gate, taps, ids, halo_ids, halo, gain, shift, out, ext, moved, depth):
    positions = value.shape[0]
    width = taps.shape[0]

    @pl.when(pl.program_id(0) == 0)
    def _():
        own = ids[...].astype(F32)
        own8 = jnp.broadcast_to(own, (8, positions))
        column = jnp.transpose(own8)[:, 0:1]
        t = lax.broadcasted_iota(jnp.int32, (positions, positions), 0)
        s = lax.broadcasted_iota(jnp.int32, (positions, positions), 1)
        near = (column == own) & (s < t) & (s > t - width)
        t = lax.broadcasted_iota(jnp.int32, (positions, 128), 0)
        s = lax.broadcasted_iota(jnp.int32, (positions, 128), 1)
        behind = (column == halo_ids[0:1, :].astype(F32)) & (s - 128 > t - width)
        count = jnp.dot(
            near.astype(F32).astype(BF16), jnp.ones((positions, 128), BF16), preferred_element_type=F32
        )
        count = count + jnp.dot(
            behind.astype(F32).astype(BF16), jnp.ones((128, 128), BF16), preferred_element_type=F32
        )
        depth[...] = count

    ext[0:HALO, :] = halo[0:HALO, :].astype(F32)
    ext[HALO : HALO + positions, :] = glu_of(value[...], gate[...]).astype(F32)
    ext[HALO + positions :, :] = jnp.zeros((8, 128), F32)
    span = HALO + positions
    for r in range(1, 8):
        moved[r, :, :] = ext[pl.ds(r, span), :]
    rows = 64
    for base in range(0, positions, rows):
        deep = depth[base : base + rows, :]
        total = jnp.zeros((rows, 128), F32)
        for i in range(width):
            start = HALO - (width - 1) + i
            r = start % 8
            at = base + start - r
            x = ext[at : at + rows, :] if r == 0 else moved[r, at : at + rows, :]
            term = taps[i : i + 1, :].astype(F32) * x
            lag = width - 1 - i
            total = total + (jnp.where(deep >= lag, term, 0.0) if lag else term)
        mean = jnp.mean(total, axis=-1, keepdims=True)
        centered = total - mean
        var = jnp.mean(centered * centered, axis=-1, keepdims=True)
        v = centered * lax.rsqrt(var + EPS) * gain[...] + shift[...]
        out[base : base + rows, :] = jax.nn.silu(v).astype(BF16)


def spread_kernel(act, conv_out, residual, norm_gain, routes, weights, stream, normed, outgoing, meta, wide):
    step = pl.program_id(0)
    tokens = act.shape[1]
    half_in = act.shape[2]
    columns = conv_out.shape[1]
    steps = wide.shape[0]
    part = jnp.dot(act[0], conv_out[0:half_in, :], preferred_element_type=F32)
    part = part + jnp.dot(act[1], conv_out[half_in:, :], preferred_element_type=F32)
    wide[step] = (residual[...].astype(F32) + part).astype(BF16).astype(F32)

    @pl.when(step == steps - 1)
    def _():
        blocks = [wide[n] for n in range(steps)]
        square = sum(jnp.sum(b * b, axis=-1, keepdims=True) for b in blocks)
        model_width = columns * steps
        scale = lax.rsqrt(square / model_width + EPS)
        for n, b in enumerate(blocks):
            at = n * columns
            stream[:, at : at + columns] = b.astype(BF16)
            normed[:, at : at + columns] = (b * scale * norm_gain[:, at : at + columns]).astype(BF16)
        experts = outgoing.shape[0] // 8
        expert = lax.broadcasted_iota(jnp.int32, (experts, tokens), 0)
        hot = [(expert == routes[k : k + 1, :]).astype(F32) for k in range(2)]
        a = lax.broadcasted_iota(jnp.int32, (tokens, tokens), 0)
        b = lax.broadcasted_iota(jnp.int32, (tokens, tokens), 1)
        before = (a < b).astype(F32).astype(BF16)
        ahead = [jnp.dot(h.astype(BF16), before, preferred_element_type=F32) for h in hot]
        ahead[1] = ahead[1] + jnp.sum(hot[0], axis=1, keepdims=True)
        slot = [jnp.sum(h * c, axis=0, keepdims=True) for h, c in zip(hot, ahead)]
        target = [routes[k : k + 1, :].astype(F32) * 4.0 + slot[k] for k in range(2)]
        meta[...] = jnp.concatenate(
            target + [weights[0:1, :], weights[1:2, :], jnp.zeros((4, tokens), F32)], axis=0
        )
        r = lax.broadcasted_iota(jnp.int32, (8 * experts, tokens), 0)
        slots = ((r // 8) * 4 + r % 4).astype(F32)
        half = (r // 4) % 2
        chosen = (slots == target[0]) | (slots == target[1])
        pick = jnp.concatenate(
            [(chosen & (half == h)).astype(F32).astype(BF16) for h in range(2)], axis=1
        )
        mid = model_width // 2
        source = jnp.concatenate([normed[:, 0:mid], normed[:, mid:]], axis=0)
        outgoing[...] = jnp.dot(pick, source, preferred_element_type=F32).astype(BF16)


def expert_kernel(x, gate, up, down, out):
    rows, half = x.shape
    quads = rows // 16
    wide = x[...].astype(F32).reshape(quads, 2, 8, half)
    a, b = wide[:, 0], wide[:, 1]
    low = lax.broadcasted_iota(jnp.int32, (quads, 8, half), 1) < 4
    top = jnp.where(low, a, pltpu.roll(b, 4, 1)).reshape(quads * 8, half).astype(BF16)
    bottom = jnp.where(low, pltpu.roll(a, 4, 1), b).reshape(quads * 8, half).astype(BF16)

    def apply(w):
        return jnp.dot(top, w[0:half, :], preferred_element_type=F32) + jnp.dot(
            bottom, w[half:, :], preferred_element_type=F32
        )

    hidden = (jax.nn.silu(apply(gate)) * apply(up)).astype(BF16)
    left = jnp.dot(hidden, down[:, 0:half], preferred_element_type=F32).reshape(quads, 8, half)
    right = jnp.dot(hidden, down[:, half:], preferred_element_type=F32).reshape(quads, 8, half)
    first = jnp.where(low, left, pltpu.roll(right, 4, 1))
    second = jnp.where(low, pltpu.roll(left, 4, 1), right)
    out[...] = jnp.stack([first, second], axis=1).reshape(rows, half).astype(BF16)


def shared_kernel(normed, gate, up, down, out):
    rows = normed[...]
    g = jnp.dot(rows, gate[...], preferred_element_type=F32)
    u = jnp.dot(rows, up[...], preferred_element_type=F32)
    hidden = (jax.nn.silu(g) * u).astype(BF16)
    part = jnp.dot(hidden, down[...], preferred_element_type=F32)

    @pl.when(pl.program_id(0) == 0)
    def _():
        out[...] = part

    @pl.when(pl.program_id(0) > 0)
    def _():
        out[...] += part


def gather_kernel(returned, meta, stream, shared, out):
    rows, half = returned.shape
    tokens = stream.shape[0]
    columns = jnp.transpose(meta[...])
    r = lax.broadcasted_iota(jnp.int32, (tokens, rows), 1)
    slots = ((r // 8) * 4 + r % 4).astype(F32)
    side = (r // 4) % 2
    weight = jnp.where(
        slots == columns[:, 0:1],
        columns[:, 2:3],
        jnp.where(slots == columns[:, 1:2], columns[:, 3:4], 0.0),
    )
    high = weight.astype(BF16)
    low = (weight - high.astype(F32)).astype(BF16)
    zero = jnp.zeros_like(weight)
    for h in range(2):
        at = h * half
        here = side == h
        first = jnp.where(here, high.astype(F32), zero).astype(BF16)
        second = jnp.where(here, low.astype(F32), zero).astype(BF16)
        routed = jnp.dot(first, returned[...], preferred_element_type=F32) + jnp.dot(
            second, returned[...], preferred_element_type=F32
        )
        base = stream[:, at : at + half].astype(F32) + shared[:, at : at + half]
        out[:, at : at + half] = (base + routed).astype(BF16)


def full(shape):
    zeros = (0,) * len(shape)
    return pl.BlockSpec(shape, lambda *_: zeros)


def per_device(
    conv_value,
    conv_gate,
    taps,
    doc_ids,
    gn_gain,
    gn_shift,
    conv_out,
    residual,
    norm_gain,
    routes,
    route_weight,
    expert_gate,
    expert_up,
    expert_down,
    shared_gate,
    shared_up,
    shared_down,
):
    positions, channels = conv_value.shape
    width = taps.shape[0]
    tokens, model_width = residual.shape
    experts = expert_gate.shape[0] * lax.axis_size("sp") * lax.axis_size("tp")
    half = model_width // 2
    ids = doc_ids.reshape(1, positions)
    sds = jax.ShapeDtypeStruct

    last = positions // HALO - 1
    packed = pl.pallas_call(
        pack_kernel,
        grid=(1,),
        in_specs=[
            pl.BlockSpec((HALO, channels), lambda i: (last, 0)),
            pl.BlockSpec((HALO, channels), lambda i: (last, 0)),
            full((1, positions)),
        ],
        out_specs=full((PACK, channels)),
        out_shape=sds((PACK, channels), BF16),
        name="pack",
    )(conv_value, conv_gate, ids)
    halo = from_behind(packed, "sp", 1)

    act = pl.pallas_call(
        conv_kernel,
        grid=(channels // 128,),
        in_specs=[
            pl.BlockSpec((positions, 128), lambda i: (0, i)),
            pl.BlockSpec((positions, 128), lambda i: (0, i)),
            pl.BlockSpec((width, 128), lambda i: (0, i)),
            full((1, positions)),
            pl.BlockSpec((8, 128), lambda i: (HALO // 8, 0)),
            pl.BlockSpec((HALO, 128), lambda i: (0, i)),
            pl.BlockSpec((1, 128), lambda i: (0, i)),
            pl.BlockSpec((1, 128), lambda i: (0, i)),
        ],
        out_specs=pl.BlockSpec((positions, 128), lambda i: (0, i)),
        out_shape=sds((positions, channels), BF16),
        scratch_shapes=[
            pltpu.VMEM((HALO + positions + 8, 128), F32),
            pltpu.VMEM((8, HALO + positions, 128), F32),
            pltpu.VMEM((positions, 128), F32),
        ],
        name="conv",
    )(
        conv_value,
        conv_gate,
        taps,
        ids,
        halo,
        halo,
        gn_gain.reshape(1, channels),
        gn_shift.reshape(1, channels),
    )
    both = lax.all_to_all(
        act.reshape(2, tokens, channels), "tp", split_axis=0, concat_axis=0, tiled=True
    )

    steps = 4
    block = model_width // steps
    stream, normed, outgoing, meta = pl.pallas_call(
        spread_kernel,
        grid=(steps,),
        in_specs=[
            full((2, tokens, channels)),
            pl.BlockSpec((2 * channels, block), lambda i: (0, i)),
            pl.BlockSpec((tokens, block), lambda i: (0, i)),
            full((1, model_width)),
            full((2, tokens)),
            full((2, tokens)),
        ],
        out_specs=[
            full((tokens, model_width)),
            full((tokens, model_width)),
            full((8 * experts, half)),
            full((8, tokens)),
        ],
        out_shape=[
            sds((tokens, model_width), BF16),
            sds((tokens, model_width), BF16),
            sds((8 * experts, half), BF16),
            sds((8, tokens), F32),
        ],
        scratch_shapes=[pltpu.VMEM((steps, tokens, block), F32)],
        name="spread",
    )(both, conv_out, residual, norm_gain.reshape(1, model_width), routes.T, route_weight.T)

    exchange = functools.partial(
        lax.all_to_all, axis_name=("sp", "tp"), split_axis=0, concat_axis=0, tiled=True
    )
    arrived = exchange(outgoing.reshape(experts, 8, half)).reshape(8 * experts, half)

    hidden = shared_gate.shape[1]
    piece = 128
    shared = pl.pallas_call(
        shared_kernel,
        grid=(hidden // piece,),
        in_specs=[
            full((tokens, model_width)),
            pl.BlockSpec((model_width, piece), lambda i: (0, i)),
            pl.BlockSpec((model_width, piece), lambda i: (0, i)),
            pl.BlockSpec((piece, model_width), lambda i: (i, 0)),
        ],
        out_specs=full((tokens, model_width)),
        out_shape=sds((tokens, model_width), F32),
        cost_estimate=pl.CostEstimate(flops=8_000_000_000, bytes_accessed=8_000_000, transcendentals=0),
        name="shared",
    )(normed, shared_gate, shared_up, shared_down)

    hidden = expert_gate.shape[2]
    chunk = 2 * experts
    result = pl.pallas_call(
        expert_kernel,
        grid=(8 * experts // chunk,),
        in_specs=[
            pl.BlockSpec((chunk, half), lambda i: (i, 0)),
            full((model_width, hidden)),
            full((model_width, hidden)),
            full((hidden, model_width)),
        ],
        out_specs=pl.BlockSpec((chunk, half), lambda i: (i, 0)),
        out_shape=sds((8 * experts, half), BF16),
        name="expert",
    )(arrived, expert_gate[0], expert_up[0], expert_down[0])
    returned = exchange(result.reshape(experts, 8, half)).reshape(8 * experts, half)

    return pl.pallas_call(
        gather_kernel,
        out_shape=sds((tokens, model_width), BF16),
        name="gather",
    )(returned, meta, stream, shared)


def solution(mesh):
    return jax.shard_map(
        per_device,
        mesh=mesh,
        in_specs=(
            P("sp", "tp"),
            P("sp", "tp"),
            P(None, "tp"),
            P("sp"),
            P("tp"),
            P("tp"),
            P(),
            P(("sp", "tp"), None),
            P(),
            P(("sp", "tp"), None),
            P(("sp", "tp"), None),
            P(("sp", "tp"), None, None),
            P(("sp", "tp"), None, None),
            P(("sp", "tp"), None, None),
            P(),
            P(),
            P(),
        ),
        out_specs=P(("sp", "tp"), None),
        check_vma=False,
    )
```

time: 153 us -> 118 us (0.77)
  local copies, waits for them, and re-layouts: 34.7 us -> 1.95 us
  Pallas kernels: 0 us -> 32.5 us
  matrix products: 21.1 us -> 0 us
  other arithmetic: 10 us -> 0 us
  starting transfers between devices: 12.6 us -> 8.34 us
  blocking collectives: 45.2 us -> 48.6 us
  waiting for transfers between devices: 28.2 us -> 25.5 us
    pallas_call x0 -> x6, Pallas kernels: none -> 32.5 us  [the longest x1 8.49 us: per_device(): pl.pallas_call(expert_kernel, grid=(8 * experts // chunk,), in_specs=[pl....]
    dot_general x5 -> x0, matrix products: 21.1 us -> none  [the longest x1 6.22 us: per_device(): jnp.dot(hidden, expert_down[0], preferred_element_type=jnp.float32)]
    reshape x4 -> x0, local copies, waits for them, and re-layouts: 9.99 us -> none  [the longest x2 5.71 us: per_device(): returned.reshape(experts * capacity, model_width)[target]]
    gather x2 -> x0, local copies, waits for them, and re-layouts: 8.51 us -> none  [the longest x1 5.21 us: per_device(): returned.reshape(experts * capacity, model_width)[target]]
    another operation x5 -> x0, local copies, waits for them, and re-layouts: 8.07 us -> none  [the longest x1 4.1 us: per_device(): jnp.stack(results, axis=1)]
    all_to_all x1, waiting for transfers between devices: 28.2 us -> 24.1 us  [per_device(): exchange(result.reshape(experts, 8, half)).reshape(8 * experts, half)]
    add x1 -> x0, other arithmetic: 4.03 us -> none  [per_device(): conv_sum = conv_sum + jnp.where(same_doc, tap_term, 0.0)]
    slice x3 -> x0, local copies, waits for them, and re-layouts: 3.41 us -> none  [the longest x1 2.49 us: per_device(): picked[:, route_index].astype(jnp.float32)]
  transfers between devices with their start and end apart: 3 -> 2, of which waited for: 1 -> 2; matrix products, arithmetic and copies ran while one was open for 6% -> 0% of each run, Pallas kernels for 0% -> 6%
where the time goes in v1:
time: 118 us; the launch traced here: 117 us
  blocking collectives  48.6 us (41%)
  Pallas kernels  32.5 us (28%)
  waiting for transfers between devices  25.5 us (22%)
  starting transfers between devices  8.34 us (7%)
  local copies, waits for them, and re-layouts  1.95 us (2%)
    all_to_all x1, blocking collectives, per_device(): exchange(outgoing.reshape(experts, 8, half)).reshape(8 * experts, half)  41.7 us
    all_to_all x1, waiting for transfers between devices, per_device(): exchange(result.reshape(experts, 8, half)).reshape(8 * experts, half)  24.1 us
    pallas_call x1, Pallas kernels, per_device(): pl.pallas_call(expert_kernel, grid=(8 * experts // chunk,), in_specs=[pl....  8.49 us
    all_to_all x1, blocking collectives, per_device(): lax.all_to_all(act.reshape(2, tokens, channels), 'tp', split_axis=0, conc...  6.94 us
    pallas_call x1, Pallas kernels, per_device(): pl.pallas_call(shared_kernel, grid=(hidden // piece,), in_specs=[full((to...  6.51 us
    pallas_call x1, Pallas kernels, per_device(): pl.pallas_call(spread_kernel, grid=(steps,), in_specs=[full((2, tokens, c...  6.35 us
    pallas_call x1, Pallas kernels, per_device(): pl.pallas_call(conv_kernel, grid=(channels // 128,), in_specs=[pl.BlockSp...  5.41 us
    all_to_all x1, starting transfers between devices, per_device(): exchange(result.reshape(experts, 8, half)).reshape(8 * experts, half)  4.42 us
  transfers between devices with their start and end apart: 2, of which 2 were waited for; matrix products, arithmetic and copies ran while one was open for 0% of the time, Pallas kernels for 6%

profile of v1, /device:TPU:1, one launch (start us, length us, event | category | flops | bytes accessed | tf_op | source)
XLA Modules:
  0.0 116.9 jit_solution(5766758515567620845)
XLA Ops:
  0.0 1.4 %pack.1 = bf16[40,512]{1,0:T(8,128)(2,1)} custom-call(bf16[256,512]{1,0:T(8,128)(2,1)} %value.3, bf16[256,512]{1,0:T(8,128)(2,1)} %gate.4, s32[1,256]{1,0:T(1,128)} %bitcast.23), custom_call_target="tpu_custom_call" | custom-call | tf_op jit(solution)/shard_map/pack/pallas_call | solution.py:229
  1.4 3.9 %collective-permute-start = (bf16[40,512]{1,0:T(8,128)(2,1)}, bf16[40,512]{1,0:T(8,128)(2,1)S(1)}, u32[]{:S(2)}, u32[]{:S(2)}) collective-permute-start(bf16[40,512]{1,0:T(8,128)(2,1)} %pack.1), channel_id=1, source_target_pairs={{0,2},{2,4},{4,6},{6,8},{8,10},{10,12},{12,14},{14,16},{16,18},{18... | collective-permute-start | bytes 122888 | tf_op jit(solution)/shard_map/ppermute | solution.py:21
  5.3 1.4 %collective-permute-done.halo_ids.halo = bf16[40,512]{1,0:T(8,128)(2,1)S(1)} collective-permute-done((bf16[40,512]{1,0:T(8,128)(2,1)}, bf16[40,512]{1,0:T(8,128)(2,1)S(1)}, u32[]{:S(2)}, u32[]{:S(2)}) %collective-permute-start) | collective-permute-done | bytes 40992 | tf_op jit(solution)/shard_map/ppermute | solution.py:21
  6.7 0.0 copy-start.1
  6.7 0.6 copy-done.1
  7.4 5.4 %conv.1 = bf16[256,512]{1,0:T(8,128)(2,1)} custom-call(bf16[256,512]{1,0:T(8,128)(2,1)} %value.3, bf16[256,512]{1,0:T(8,128)(2,1)} %gate.4, bf16[31,512]{1,0:T(8,128)(2,1)} %taps.1, s32[1,256]{1,0:T(1,128)} %bitcast.24, bf16[40,512]{1,0:T(8,128)(2,1)} %copy-done.1, bf16[40,512]{1,0:T(8,128)(2,1)} %copy-done.1, f32[1,512]{1,0:T(1,128)} %bitcast.25, ...), custom_call_target="tpu_custom_call" | custom-call | tf_op jit(solution)/shard_map/conv/pallas_call | solution.py:243
  12.8 6.9 %all_to_all.15.act = bf16[2,128,512]{2,1,0:T(8,128)(2,1)} all-to-all(bf16[2,128,512]{2,1,0:T(8,128)(2,1)} %bitcast.21), channel_id=1, replica_groups=mesh['sp'=64,'tp'=2] {'tp'}, dimensions={0} | all-to-all | bytes 524288 | tf_op jit(solution)/shard_map/all_to_all | solution.py:274
  19.7 6.3 %spread.1 = (bf16[128,2048]{1,0:T(8,128)(2,1)}, bf16[128,2048]{1,0:T(8,128)(2,1)}, bf16[1024,1024]{1,0:T(8,128)(2,1)}, f32[8,128]{1,0:T(8,128)}) custom-call(bf16[2,128,512]{2,1,0:T(8,128)(2,1)} %all_to_all.15.act, bf16[1024,2048]{1,0:T(8,128)(2,1)} %conv_out.1, bf16[128,2048]{1,0:T(8,128)(2,1)} %residual.1, f32[1,2048]{1,0:T(1,128)} %bitcast.22, ...), custom_call_target="tpu_custom_call" | custom-call | tf_op jit(solution)/shard_map/spread/pallas_call | solution.py:280
  26.1 41.7 %all_to_all.16 = bf16[128,8,1024]{2,1,0:T(8,128)(2,1)} all-to-all(bf16[128,8,1024]{2,1,0:T(8,128)(2,1)} %bitcast.20), channel_id=1, replica_groups=mesh['sp'=64,'tp'=2] {'sp','tp'}, dimensions={0} | all-to-all | bytes 4194304 | tf_op jit(solution)/shard_map/all_to_all | solution.py:310
  67.7 8.5 %expert.1 = bf16[1024,1024]{1,0:T(8,128)(2,1)} custom-call(bf16[1024,1024]{1,0:T(8,128)(2,1)} %bitcast.15, bf16[2048,512]{1,0:T(8,128)(2,1)} %bitcast.17, bf16[2048,512]{1,0:T(8,128)(2,1)} %bitcast.18, bf16[512,2048]{1,0:T(8,128)(2,1)} %bitcast.19), custom_call_target="tpu_custom_call" | custom-call | tf_op jit(solution)/shard_map/expert/pallas_call | solution.py:331
  76.2 4.4 %all-to-all-start.2 = ((bf16[128,8,1024]{2,1,0:T(8,128)(2,1)}), bf16[128,8,1024]{2,1,0:T(8,128)(2,1)S(1)}, u32[]{:S(2)}, u32[]{:S(2)}) async-start(bf16[128,8,1024]{2,1,0:T(8,128)(2,1)} %bitcast.14), calls=%async_computation.2 | async-start | bytes 4194304 | tf_op jit(solution)/shard_map/all_to_all | solution.py:344
  80.6 6.5 %shared.1 = f32[128,2048]{1,0:T(8,128)} custom-call(bf16[128,2048]{1,0:T(8,128)(2,1)} %get-tuple-element.12.normed, bf16[2048,512]{1,0:T(8,128)(2,1)} %gate.5, bf16[2048,512]{1,0:T(8,128)(2,1)} %up.1, bf16[512,2048]{1,0:T(8,128)(2,1)} %down.1), custom_call_target="tpu_custom_call" | custom-call | flops 8000000000 | bytes 8000000 | tf_op jit(solution)/shard_map/shared/pallas_call | solution.py:314
  87.1 24.1 %all-to-all-done.2 = bf16[128,8,1024]{2,1,0:T(8,128)(2,1)S(1)} async-done(((bf16[128,8,1024]{2,1,0:T(8,128)(2,1)}), bf16[128,8,1024]{2,1,0:T(8,128)(2,1)S(1)}, u32[]{:S(2)}, u32[]{:S(2)}) %all-to-all-start.2) | async-done | bytes 2097184 | tf_op jit(solution)/shard_map/all_to_all | solution.py:344
  111.2 0.0 copy-start
  111.2 1.3 %copy-done = bf16[128,8,1024]{2,1,0:T(8,128)(2,1)} copy-done((bf16[128,8,1024]{2,1,0:T(8,128)(2,1)}, bf16[128,8,1024]{2,1,0:T(8,128)(2,1)S(1)}, u32[]{:S(2)}) %copy-start) | copy-done | bytes 2097176
  112.6 4.3 %gather.1 = bf16[128,2048]{1,0:T(8,128)(2,1)} custom-call(bf16[1024,1024]{1,0:T(8,128)(2,1)} %bitcast.16, f32[8,128]{1,0:T(8,128)} %get-tuple-element.10.meta, bf16[128,2048]{1,0:T(8,128)(2,1)} %get-tuple-element.11.stream, f32[128,2048]{1,0:T(8,128)} %shared.1), custom_call_target="tpu_custom_call" | custom-call | tf_op jit(solution)/shard_map/gather/pallas_call | solution.py:346
Async XLA Ops:
  1.4 5.3 %collective-permute-start = (bf16[40,512]{1,0:T(8,128)(2,1)}, bf16[40,512]{1,0:T(8,128)(2,1)S(1)}, u32[]{:S(2)}, u32[]{:S(2)}) collective-permute-start(bf16[40,512]{1,0:T(8,128)(2,1)} %pack.1), channel_id=1, source_target_pairs={{0,2},{2,4},{4,6},{6,8},{8,10},{10,12},{12,14},{14,16},{16,18},{18... | collective-permute-start | bytes 122888 | tf_op jit(solution)/shard_map/ppermute | solution.py:21
  6.7 0.6 copy-start.1
  76.2 35.0 %all-to-all-start.2 = ((bf16[128,8,1024]{2,1,0:T(8,128)(2,1)}), bf16[128,8,1024]{2,1,0:T(8,128)(2,1)S(1)}, u32[]{:S(2)}, u32[]{:S(2)}) async-start(bf16[128,8,1024]{2,1,0:T(8,128)(2,1)} %bitcast.14), calls=%async_computation.2 | async-start | bytes 4194304 | tf_op jit(solution)/shard_map/all_to_all | solution.py:344
  111.2 1.3 %copy-start = (bf16[128,8,1024]{2,1,0:T(8,128)(2,1)}, bf16[128,8,1024]{2,1,0:T(8,128)(2,1)S(1)}, u32[]{:S(2)}) copy-start(bf16[128,8,1024]{2,1,0:T(8,128)(2,1)S(1)} %all-to-all-done.2) | copy-start | bytes 6291460

commit v2 on v0

v2 whole, which is shorter than its diff:
```python
import functools

import jax
import jax.numpy as jnp
from jax import lax
from jax.experimental import pallas as pl
from jax.experimental.pallas import tpu as pltpu
from jax.sharding import PartitionSpec as P

GROUPS = 8
EPS = 1e-06
F32 = jnp.float32
BF16 = jnp.bfloat16
HALO = 32
PACK = 40


def from_behind(x, axis, by):
    peers = lax.axis_size(axis)
    pairs = [(i, (i + by) % peers) for i in range(peers)]
    return lax.ppermute(x, axis, pairs)


def glu_of(value, gate):
    wide = value.astype(F32) * jax.nn.sigmoid(gate.astype(F32))
    return wide.astype(BF16)


def pack_kernel(value, gate, ids, out):
    channels = value.shape[1]
    positions = ids.shape[1]
    out[0:HALO, :] = glu_of(value[...], gate[...])
    tail = ids[:, positions - 128 :].astype(F32)
    row = jnp.concatenate([tail, jnp.zeros((1, channels - 128), F32)], axis=1)
    out[HALO:, :] = jnp.broadcast_to(row, (PACK - HALO, channels)).astype(BF16)


def same_document(column, row, first, behind, width):
    shape = (column.shape[0], row.shape[1])
    t = lax.broadcasted_iota(jnp.int32, shape, 0) + first
    s = lax.broadcasted_iota(jnp.int32, shape, 1) - behind
    near = (column == row) & (s < t) & (s > t - width)
    ones = jnp.ones((shape[1], 128), BF16)
    return jnp.dot(near.astype(F32).astype(BF16), ones, preferred_element_type=F32)


def column_of(row):
    return jnp.transpose(jnp.broadcast_to(row, (8, row.shape[1])))[:, 0:1]


def normalized(fetch, deep, taps, gain, shift, lanes):
    width = taps.shape[0]
    total = jnp.zeros(deep.shape, F32)
    for i in range(width):
        term = taps[i : i + 1, lanes].astype(F32) * fetch(i)
        lag = width - 1 - i
        total = total + (jnp.where(deep >= lag, term, 0.0) if lag else term)
    mean = jnp.mean(total, axis=-1, keepdims=True)
    centered = total - mean
    var = jnp.mean(centered * centered, axis=-1, keepdims=True)
    v = centered * lax.rsqrt(var + EPS) * gain[:, lanes] + shift[:, lanes]
    return jax.nn.silu(v).astype(BF16)


def conv_kernel(value, gate, taps, ids, gain, shift, act, ext, moved, depth):
    positions, channels = value.shape
    width = taps.shape[0]
    own = ids[...].astype(F32)
    depth[...] = same_document(column_of(own), own, 0, 0, width)
    ext[positions:, :] = jnp.zeros((8, 128), F32)
    for c in range(channels // 128):
        lanes = slice(c * 128, c * 128 + 128)
        ext[0:positions, :] = glu_of(value[:, lanes], gate[:, lanes]).astype(F32)
        for r in range(1, 8):
            moved[r, :, :] = ext[pl.ds(r, positions), :]
        base = HALO
        while base < positions:
            rows = HALO if base == HALO else 2 * HALO

            def fetch(i, base=base, rows=rows):
                start = base - (width - 1) + i
                r = start % 8
                at = slice(start - r, start - r + rows)
                return ext[at, :] if r == 0 else moved[r, at, :]

            deep = depth[base : base + rows, :]
            act[base : base + rows, lanes] = normalized(fetch, deep, taps, gain, shift, lanes)
            base += rows


def rim_kernel(act, value, gate, taps, ids, halo, gain, shift, keep, send, ext, moved):
    channels = value.shape[1]
    rows = HALO
    width = taps.shape[0]
    tokens = keep.shape[0]
    mine = lax.axis_index("tp")
    own = ids[...].astype(F32)
    column = column_of(own)[0:rows]
    deep = same_document(column, own, 0, 0, width) + same_document(
        column, halo[HALO : HALO + 1, 0:128].astype(F32), 0, 128, width
    )
    at = pl.multiple_of(mine * tokens, tokens)
    keep[...] = act[pl.ds(at, tokens), :]
    at = pl.multiple_of((1 - mine) * tokens, tokens)
    send[...] = act[pl.ds(at, tokens), :]
    ext[2 * HALO :, :] = jnp.zeros((8, 128), F32)
    for c in range(channels // 128):
        lanes = slice(c * 128, c * 128 + 128)
        ext[0:HALO, :] = halo[0:HALO, lanes].astype(F32)
        ext[HALO : 2 * HALO, :] = glu_of(value[0:rows, lanes], gate[0:rows, lanes]).astype(F32)
        for r in range(1, 8):
            moved[r, :, :] = ext[pl.ds(r, 2 * HALO), :]

        def fetch(i):
            start = HALO - (width - 1) + i
            r = start % 8
            at = slice(start - r, start - r + rows)
            return ext[at, :] if r == 0 else moved[r, at, :]

        first = normalized(fetch, deep, taps, gain, shift, lanes)

        @pl.when(mine == 0)
        def _():
            keep[0:rows, lanes] = first

        @pl.when(mine == 1)
        def _():
            send[0:rows, lanes] = first


def route_kernel(routes, weights, meta, pick):
    tokens = routes.shape[1]
    experts = pick.shape[0] // 8
    expert = lax.broadcasted_iota(jnp.int32, (experts, tokens), 0)
    hot = [(expert == routes[k : k + 1, :]).astype(F32) for k in range(2)]
    a = lax.broadcasted_iota(jnp.int32, (tokens, tokens), 0)
    b = lax.broadcasted_iota(jnp.int32, (tokens, tokens), 1)
    before = (a < b).astype(F32).astype(BF16)
    ahead = [jnp.dot(h.astype(BF16), before, preferred_element_type=F32) for h in hot]
    ahead[1] = ahead[1] + jnp.sum(hot[0], axis=1, keepdims=True)
    slot = [jnp.sum(h * c, axis=0, keepdims=True) for h, c in zip(hot, ahead)]
    target = [routes[k : k + 1, :].astype(F32) * 4.0 + slot[k] for k in range(2)]
    meta[...] = jnp.concatenate(
        target + [weights[0:1, :], weights[1:2, :], jnp.zeros((4, tokens), F32)], axis=0
    )
    r = lax.broadcasted_iota(jnp.int32, (8 * experts, tokens), 0)
    slots = ((r // 8) * 4 + r % 4).astype(F32)
    half = (r // 4) % 2
    chosen = (slots == target[0]) | (slots == target[1])
    for h in range(2):
        pick[:, h * tokens : (h + 1) * tokens] = (chosen & (half == h)).astype(F32).astype(BF16)


def spread_kernel(keep, got, conv_out, residual, norm_gain, pick, stream, normed, outgoing):
    tokens, half_in = keep.shape
    model_width = residual.shape[1]
    mine = lax.axis_index("tp")
    first = pl.multiple_of(mine * half_in, half_in)
    other = pl.multiple_of((1 - mine) * half_in, half_in)
    part = jnp.dot(keep[...], conv_out[pl.ds(first, half_in), :], preferred_element_type=F32)
    part = part + jnp.dot(got[...], conv_out[pl.ds(other, half_in), :], preferred_element_type=F32)
    rows = (residual[...].astype(F32) + part).astype(BF16)
    stream[...] = rows
    wide = rows.astype(F32)
    scale = lax.rsqrt(jnp.mean(wide * wide, axis=-1, keepdims=True) + EPS)
    ready = (wide * scale * norm_gain[...]).astype(BF16)
    normed[...] = ready
    mid = model_width // 2
    source = jnp.concatenate([ready[:, 0:mid], ready[:, mid:]], axis=0)
    outgoing[...] = jnp.dot(pick[...], source, preferred_element_type=F32).astype(BF16)


def expert_kernel(x, gate, up, down, out):
    rows, half = out.shape
    at = pl.ds(pl.multiple_of(pl.program_id(0) * rows, rows), rows)
    quads = rows // 16
    wide = x[at, :].astype(F32).reshape(quads, 2, 8, half)
    a, b = wide[:, 0], wide[:, 1]
    low = lax.broadcasted_iota(jnp.int32, (quads, 8, half), 1) < 4
    top = jnp.where(low, a, pltpu.roll(b, 4, 1)).reshape(quads * 8, half).astype(BF16)
    bottom = jnp.where(low, pltpu.roll(a, 4, 1), b).reshape(quads * 8, half).astype(BF16)

    def apply(w):
        return jnp.dot(top, w[0:half, :], preferred_element_type=F32) + jnp.dot(
            bottom, w[half:, :], preferred_element_type=F32
        )

    hidden = (jax.nn.silu(apply(gate)) * apply(up)).astype(BF16)
    left = jnp.dot(hidden, down[:, 0:half], preferred_element_type=F32).reshape(quads, 8, half)
    right = jnp.dot(hidden, down[:, half:], preferred_element_type=F32).reshape(quads, 8, half)
    first = jnp.where(low, left, pltpu.roll(right, 4, 1))
    second = jnp.where(low, pltpu.roll(left, 4, 1), right)
    out[...] = jnp.stack([first, second], axis=1).reshape(rows, half).astype(BF16)


def shared_kernel(normed, stream, gate, up, down, out):
    rows = normed[...]
    g = jnp.dot(rows, gate[...], preferred_element_type=F32)
    u = jnp.dot(rows, up[...], preferred_element_type=F32)
    hidden = (jax.nn.silu(g) * u).astype(BF16)
    part = jnp.dot(hidden, down[...], preferred_element_type=F32)

    @pl.when(pl.program_id(0) == 0)
    def _():
        out[...] = stream[...].astype(F32) + part

    @pl.when(pl.program_id(0) > 0)
    def _():
        out[...] += part


def gather_kernel(returned, meta, base, out):
    rows, half = returned.shape
    tokens = base.shape[0]
    h = pl.program_id(0)
    columns = jnp.transpose(meta[...])
    r = lax.broadcasted_iota(jnp.int32, (tokens, rows), 1)
    slots = ((r // 8) * 4 + r % 4).astype(F32)
    here = (r // 4) % 2 == h
    weight = jnp.where(
        here & (slots == columns[:, 0:1]),
        columns[:, 2:3],
        jnp.where(here & (slots == columns[:, 1:2]), columns[:, 3:4], 0.0),
    )
    high = weight.astype(BF16)
    low = (weight - high.astype(F32)).astype(BF16)
    routed = jnp.dot(high, returned[...], preferred_element_type=F32) + jnp.dot(
        low, returned[...], preferred_element_type=F32
    )
    out[...] = (base[:, pl.ds(pl.multiple_of(h * half, half), half)] + routed).astype(BF16)


def whole(shape):
    zeros = (0,) * len(shape)
    return pl.BlockSpec(shape, lambda *_: zeros)


def held(x):
    return pltpu.with_memory_space_constraint(x, pltpu.VMEM), pl.BlockSpec(memory_space=pltpu.VMEM)


def copied(x, spec=None):
    return pltpu.with_memory_space_constraint(x, pltpu.HBM), spec or whole(x.shape)


def kernel(body, name, args, outs, us, grid=1, scratch=(), room=16):
    here = pl.BlockSpec(memory_space=pltpu.VMEM)
    return pl.pallas_call(
        body,
        grid=(grid,),
        in_specs=[spec for _, spec in args],
        out_specs=[here if spec is None else spec for _, _, spec in outs],
        out_shape=[
            (pltpu.VMEM if spec is None else pltpu.HBM)(shape, dtype)
            for shape, dtype, spec in outs
        ],
        scratch_shapes=scratch,
        cost_estimate=pl.CostEstimate(flops=int(us * 1e9), bytes_accessed=1000, transcendentals=0),
        compiler_params=pltpu.CompilerParams(vmem_limit_bytes=room * 2**20),
        name=name,
    )(*[x for x, _ in args])


def per_device(
    conv_value,
    conv_gate,
    taps,
    doc_ids,
    gn_gain,
    gn_shift,
    conv_out,
    residual,
    norm_gain,
    routes,
    route_weight,
    expert_gate,
    expert_up,
    expert_down,
    shared_gate,
    shared_up,
    shared_down,
):
    positions, channels = conv_value.shape
    tokens, model_width = residual.shape
    experts = expert_gate.shape[0] * lax.axis_size("sp") * lax.axis_size("tp")
    half = model_width // 2
    ids = doc_ids.reshape(1, positions)
    gain = gn_gain.reshape(1, channels)
    shift = gn_shift.reshape(1, channels)

    last = positions // HALO - 1
    tail = pl.BlockSpec((HALO, channels), lambda i: (last, 0))
    (packed,) = kernel(
        pack_kernel,
        "pack",
        [copied(conv_value, tail), copied(conv_gate, tail), copied(ids)],
        [((PACK, channels), BF16, None)],
        us=1,
    )
    halo = from_behind(packed, "sp", 1)
    (act,) = kernel(
        conv_kernel,
        "conv",
        [held(conv_value), held(conv_gate), held(taps), held(ids), held(gain), held(shift)],
        [((positions, channels), BF16, None)],
        us=4,
        scratch=[
            pltpu.VMEM((positions + 8, 128), F32),
            pltpu.VMEM((8, positions, 128), F32),
            pltpu.VMEM((positions, 128), F32),
        ],
    )
    keep, send = kernel(
        rim_kernel,
        "rim",
        [
            held(act),
            held(conv_value),
            held(conv_gate),
            held(taps),
            held(ids),
            held(halo),
            held(gain),
            held(shift),
        ],
        [((tokens, channels), BF16, None), ((tokens, channels), BF16, None)],
        us=1,
        scratch=[pltpu.VMEM((2 * HALO + 8, 128), F32), pltpu.VMEM((8, 2 * HALO, 128), F32)],
    )
    got = lax.ppermute(send, "tp", [(0, 1), (1, 0)])
    meta, pick = kernel(
        route_kernel,
        "route",
        [held(routes.T), held(route_weight.T)],
        [((8, tokens), F32, None), ((8 * experts, 2 * tokens), BF16, None)],
        us=2,
    )
    rows = (tokens, model_width)
    stream, normed, outgoing = kernel(
        spread_kernel,
        "spread",
        [
            held(keep),
            held(got),
            held(conv_out),
            held(residual),
            held(norm_gain.reshape(1, model_width)),
            held(pick),
        ],
        [(rows, BF16, whole(rows)), (rows, BF16, whole(rows)), ((8 * experts, half), BF16, None)],
        us=3,
    )

    exchange = functools.partial(
        lax.all_to_all, axis_name=("sp", "tp"), split_axis=0, concat_axis=0, tiled=True
    )
    arrived = exchange(outgoing.reshape(experts, 8, half)).reshape(8 * experts, half)
    piece = 128
    by_column = pl.BlockSpec((model_width, piece), lambda i: (0, i))
    (base,) = kernel(
        shared_kernel,
        "shared",
        [
            copied(normed),
            copied(stream),
            copied(shared_gate, by_column),
            copied(shared_up, by_column),
            copied(shared_down, pl.BlockSpec((piece, model_width), lambda i: (i, 0))),
        ],
        [(rows, F32, None)],
        us=8,
        grid=shared_gate.shape[1] // piece,
    )
    (result,) = kernel(
        expert_kernel,
        "expert",
        [held(arrived), held(expert_gate[0]), held(expert_up[0]), held(expert_down[0])],
        [((8 * experts, half), BF16, pl.BlockSpec((2 * experts, half), lambda i: (i, 0)))],
        us=5,
        grid=4,
    )
    returned = exchange(result.reshape(experts, 8, half)).reshape(8 * experts, half)
    (out,) = kernel(
        gather_kernel,
        "gather",
        [held(returned), held(meta), held(base)],
        [(rows, BF16, pl.BlockSpec((tokens, half), lambda i: (0, i)))],
        us=2,
        grid=2,
    )
    return out


def solution(mesh):
    return jax.shard_map(
        per_device,
        mesh=mesh,
        in_specs=(
            P("sp", "tp"),
            P("sp", "tp"),
            P(None, "tp"),
            P("sp"),
            P("tp"),
            P("tp"),
            P(),
            P(("sp", "tp"), None),
            P(),
            P(("sp", "tp"), None),
            P(("sp", "tp"), None),
            P(("sp", "tp"), None, None),
            P(("sp", "tp"), None, None),
            P(("sp", "tp"), None, None),
            P(),
            P(),
            P(),
        ),
        out_specs=P(("sp", "tp"), None),
        check_vma=False,
    )
```

time: 153 us -> 95.5 us (0.62)
  local copies, waits for them, and re-layouts: 34.7 us -> 1.38 us
  matrix products: 21.1 us -> 0 us
  Pallas kernels: 0 us -> 21 us
  blocking collectives: 45.2 us -> 33.7 us
  other arithmetic: 10 us -> 0 us
  starting transfers between devices: 12.6 us -> 8.14 us
  waiting for transfers between devices: 28.2 us -> 30.9 us
    dot_general x5 -> x0, matrix products: 21.1 us -> none  [the longest x1 6.22 us: per_device(): jnp.dot(hidden, expert_down[0], preferred_element_type=jnp.float32)]
    pallas_call x0 -> x8, Pallas kernels: none -> 21 us  [kernel(): pl.pallas_call(body, grid=(grid,), in_specs=[spec for _, spec in args], o...]
    all_to_all x2 -> x1, blocking collectives: 45.2 us -> 33.7 us  [per_device(): exchange(outgoing.reshape(experts, 8, half)).reshape(8 * experts, half)]
    reshape x4 -> x0, local copies, waits for them, and re-layouts: 9.99 us -> none  [the longest x2 5.71 us: per_device(): returned.reshape(experts * capacity, model_width)[target]]
    gather x2 -> x0, local copies, waits for them, and re-layouts: 8.51 us -> none  [the longest x1 5.21 us: per_device(): returned.reshape(experts * capacity, model_width)[target]]
    another operation x5 -> x0, local copies, waits for them, and re-layouts: 8.07 us -> none  [the longest x1 4.1 us: per_device(): jnp.stack(results, axis=1)]
    ppermute x2 -> x1, waiting for transfers between devices: 0.01 us -> 5.93 us  [from_behind(): return lax.ppermute(x, axis, pairs)]
    ppermute x2 -> x1, starting transfers between devices: 7.04 us -> 2.1 us  [from_behind(): return lax.ppermute(x, axis, pairs)]
  transfers between devices with their start and end apart: 3 -> 3, of which waited for: 1 -> 3; matrix products, arithmetic and copies ran while one was open for 6% -> 0% of each run, Pallas kernels for 0% -> 10%
where the time goes in v2:
time: 95.5 us; the launch traced here: 95.3 us
  blocking collectives  33.7 us (35%)
  waiting for transfers between devices  30.9 us (32%)
  Pallas kernels  21 us (22%)
  starting transfers between devices  8.14 us (9%)
  local copies, waits for them, and re-layouts  1.38 us (1%)
    all_to_all x1, blocking collectives, per_device(): exchange(outgoing.reshape(experts, 8, half)).reshape(8 * experts, half)  33.7 us
    all_to_all x1, waiting for transfers between devices, per_device(): exchange(result.reshape(experts, 8, half)).reshape(8 * experts, half)  24.8 us
    pallas_call x8, Pallas kernels, kernel(): pl.pallas_call(body, grid=(grid,), in_specs=[spec for _, spec in args], o...  21 us
    ppermute x1, waiting for transfers between devices, from_behind(): return lax.ppermute(x, axis, pairs)  5.93 us
    all_to_all x1, starting transfers between devices, per_device(): exchange(result.reshape(experts, 8, half)).reshape(8 * experts, half)  4.41 us
    ppermute x1, starting transfers between devices, from_behind(): return lax.ppermute(x, axis, pairs)  2.1 us
  transfers between devices with their start and end apart: 3, of which 3 were waited for; matrix products, arithmetic and copies ran while one was open for 0% of the time, Pallas kernels for 10%

profile of v2, /device:TPU:1, one launch (start us, length us, event | category | flops | bytes accessed | tf_op | source)
XLA Modules:
  0.0 95.3 jit_solution(9655509291259404846)
XLA Ops:
  0.0 0.0 copy-start.6
  0.0 0.0 copy-start.5
  0.0 0.0 copy-start.11
  0.0 0.0 copy-start.7
  0.0 0.0 copy-start.10
  0.0 0.0 copy-start.9
  0.0 0.8 pack.1
  0.9 2.1 %collective-permute-start = (bf16[40,512]{1,0:T(8,128)(2,1)S(1)}, bf16[40,512]{1,0:T(8,128)(2,1)S(1)}, u32[]{:S(2)}, u32[]{:S(2)}) collective-permute-start(bf16[40,512]{1,0:T(8,128)(2,1)S(1)} %pack.1), channel_id=1, source_target_pairs={{0,2},{2,4},{4,6},{6,8},{8,10},{10,12},{12,14},{14,16},{16,18},{18... | collective-permute-start | bytes 122888 | tf_op jit(solution)/shard_map/ppermute | solution.py:21
  3.0 0.0 copy-done.6
  3.0 0.0 copy-done.5
  3.0 0.0 copy-done.11
  3.0 0.0 copy-done.7
  3.0 0.0 copy-done.10
  3.0 0.0 copy-done.9
  3.0 2.6 %conv.1.act = bf16[256,512]{1,0:T(8,128)(2,1)S(1)} custom-call(bf16[256,512]{1,0:T(8,128)(2,1)S(1)} %copy-done.5, bf16[256,512]{1,0:T(8,128)(2,1)S(1)} %copy-done.6, bf16[31,512]{1,0:T(8,128)(2,1)S(1)} %copy-done.7, s32[1,256]{1,0:T(1,128)S(1)} %bitcast.25, f32[1,512]{1,0:T(1,128)S(1)} %bitcast.20, f32[1,512]{1,0:T(1,128)S(1)} %bitcast.22), custom_call_target="tpu_custom_call" | custom-call | flops 4000000000 | bytes 1000 | tf_op jit(solution)/shard_map/conv/pallas_call | solution.py:248
  5.6 0.0 copy-start.12
  5.6 0.0 copy-start.13
  5.6 5.9 %collective-permute-done.halo = bf16[40,512]{1,0:T(8,128)(2,1)S(1)} collective-permute-done((bf16[40,512]{1,0:T(8,128)(2,1)S(1)}, bf16[40,512]{1,0:T(8,128)(2,1)S(1)}, u32[]{:S(2)}, u32[]{:S(2)}) %collective-permute-start) | collective-permute-done | bytes 40992 | tf_op jit(solution)/shard_map/ppermute | solution.py:21
  11.6 1.3 %rim.1 = (bf16[128,512]{1,0:T(8,128)(2,1)S(1)}, bf16[128,512]{1,0:T(8,128)(2,1)S(1)}) custom-call(bf16[256,512]{1,0:T(8,128)(2,1)S(1)} %conv.1.act, bf16[256,512]{1,0:T(8,128)(2,1)S(1)} %copy-done.5, bf16[256,512]{1,0:T(8,128)(2,1)S(1)} %copy-done.6, bf16[31,512]{1,0:T(8,128)(2,1)S(1)} %copy-done.7, s32[1,256]{1,0:T(1,128)S(1)} %bitcast.26, ...), custom_call_target="tpu_custom_call" | custom-call | flops 1000000000 | bytes 1000 | tf_op jit(solution)/shard_map/rim/pallas_call | solution.py:248
  12.8 1.6 %collective-permute-start.1 = (bf16[128,512]{1,0:T(8,128)(2,1)S(1)}, bf16[128,512]{1,0:T(8,128)(2,1)S(1)}, u32[]{:S(2)}, u32[]{:S(2)}) collective-permute-start(bf16[128,512]{1,0:T(8,128)(2,1)S(1)} %get-tuple-element.13), channel_id=1, source_target_pairs={{0,1},{1,0},{2,3},{3,2},{4,5},{5,4},{6,7},{7,6},{8,9},{9,8},{10,11... | collective-permute-start | bytes 393224 | tf_op jit(solution)/shard_map/ppermute | solution.py:330
  14.5 0.0 copy-done.12
  14.5 0.0 copy-done.13
  14.5 0.0 copy-start
  14.5 0.0 copy-start.4
  14.5 0.0 copy-start.8
  14.5 0.8 route.1
  15.3 0.2 collective-permute-done.1.got
  15.5 1.2 %copy-done = bf16[1024,2048]{1,0:T(8,128)(2,1)S(1)} copy-done((bf16[1024,2048]{1,0:T(8,128)(2,1)S(1)}, bf16[1024,2048]{1,0:T(8,128)(2,1)}, u32[]{:S(2)}) %copy-start) | copy-done | bytes 4194328
  16.7 0.1 copy-done.4
  16.8 0.0 copy-done.8
  16.8 0.0 copy-start.3
  16.8 1.8 %spread.1 = (bf16[128,2048]{1,0:T(8,128)(2,1)}, bf16[128,2048]{1,0:T(8,128)(2,1)}, bf16[1024,1024]{1,0:T(8,128)(2,1)S(1)}) custom-call(bf16[128,512]{1,0:T(8,128)(2,1)S(1)} %get-tuple-element.12.keep, bf16[128,512]{1,0:T(8,128)(2,1)S(1)} %collective-permute-done.1.got, bf16[1024,2048]{1,0:T(8,128)(2,1)S(1)} %copy-done, bf16[128,2048]{1,0:T(8,128)(2,1)S(1)} %copy-done.4, ...), custom_call_target="tpu_custom_call" | custom-call | flops 3000000000 | bytes 1000 | tf_op jit(solution)/shard_map/spread/pallas_call | solution.py:248
  18.6 0.0 copy-start.1
  18.6 0.0 copy-start.2
  18.6 33.7 %all_to_all.10 = bf16[128,8,1024]{2,1,0:T(8,128)(2,1)S(1)} all-to-all(bf16[128,8,1024]{2,1,0:T(8,128)(2,1)S(1)} %bitcast.14), channel_id=1, replica_groups=mesh['sp'=64,'tp'=2] {'sp','tp'}, dimensions={0} | all-to-all | bytes 4194304 | tf_op jit(solution)/shard_map/all_to_all | solution.py:357
  52.3 0.0 copy-done.3
  52.3 0.0 copy-done.1
  52.3 0.0 copy-done.2
  52.3 5.4 %expert.1 = bf16[1024,1024]{1,0:T(8,128)(2,1)} custom-call(bf16[1024,1024]{1,0:T(8,128)(2,1)S(1)} %bitcast.15, bf16[2048,512]{1,0:T(8,128)(2,1)S(1)} %bitcast.16, bf16[2048,512]{1,0:T(8,128)(2,1)S(1)} %bitcast.17, bf16[512,2048]{1,0:T(8,128)(2,1)S(1)} %bitcast.18), custom_call_target="tpu_custom_call" | custom-call | flops 5000000000 | bytes 1000 | tf_op jit(solution)/shard_map/expert/pallas_call | solution.py:248
  57.7 4.4 %all-to-all-start.1 = ((bf16[128,8,1024]{2,1,0:T(8,128)(2,1)}), bf16[128,8,1024]{2,1,0:T(8,128)(2,1)S(1)}, u32[]{:S(2)}, u32[]{:S(2)}) async-start(bf16[128,8,1024]{2,1,0:T(8,128)(2,1)} %bitcast.29), calls=%async_computation.1 | async-start | bytes 4194304 | tf_op jit(solution)/shard_map/all_to_all | solution.py:382
  62.1 5.8 %shared.1.base = f32[128,2048]{1,0:T(8,128)S(1)} custom-call(bf16[128,2048]{1,0:T(8,128)(2,1)} %get-tuple-element.17.normed, bf16[128,2048]{1,0:T(8,128)(2,1)} %get-tuple-element.18.stream, bf16[2048,512]{1,0:T(8,128)(2,1)} %gate.7, bf16[2048,512]{1,0:T(8,128)(2,1)} %up.1, bf16[512,2048]{1,0:T(8,128)(2,1)} %down.1), custom_call_target="tpu_custom_call" | custom-call | flops 8000000000 | bytes 1000 | tf_op jit(solution)/shard_map/shared/pallas_call | solution.py:248
  67.8 24.8 %all-to-all-done.1 = bf16[128,8,1024]{2,1,0:T(8,128)(2,1)S(1)} async-done(((bf16[128,8,1024]{2,1,0:T(8,128)(2,1)}), bf16[128,8,1024]{2,1,0:T(8,128)(2,1)S(1)}, u32[]{:S(2)}, u32[]{:S(2)}) %all-to-all-start.1) | async-done | bytes 2097184 | tf_op jit(solution)/shard_map/all_to_all | solution.py:382
  92.7 2.6 %gather.1 = bf16[128,2048]{1,0:T(8,128)(2,1)} custom-call(bf16[1024,1024]{1,0:T(8,128)(2,1)S(1)} %bitcast.13, f32[8,128]{1,0:T(8,128)S(1)} %get-tuple-element.16.meta, f32[128,2048]{1,0:T(8,128)S(1)} %shared.1.base), custom_call_target="tpu_custom_call" | custom-call | flops 2000000000 | bytes 1000 | tf_op jit(solution)/shard_map/gather/pallas_call | solution.py:248
Async XLA Ops:
  0.0 3.0 %copy-start.6 = (bf16[256,512]{1,0:T(8,128)(2,1)S(1)}, bf16[256,512]{1,0:T(8,128)(2,1)}, u32[]{:S(2)}) copy-start(bf16[256,512]{1,0:T(8,128)(2,1)} %gate.6) | copy-start | bytes 786436
  0.0 3.0 %copy-start.5 = (bf16[256,512]{1,0:T(8,128)(2,1)S(1)}, bf16[256,512]{1,0:T(8,128)(2,1)}, u32[]{:S(2)}) copy-start(bf16[256,512]{1,0:T(8,128)(2,1)} %value.5) | copy-start | bytes 786436
  0.0 3.0 %copy-start.11 = (s32[256]{0:T(256)S(1)}, s32[256]{0:T(256)}, u32[]{:S(2)}) copy-start(s32[256]{0:T(256)} %param.20) | copy-start | bytes 3076
  0.0 3.0 %copy-start.7 = (bf16[31,512]{1,0:T(8,128)(2,1)S(1)}, bf16[31,512]{1,0:T(8,128)(2,1)}, u32[]{:S(2)}) copy-start(bf16[31,512]{1,0:T(8,128)(2,1)} %taps.3) | copy-start | bytes 95236
  0.0 3.0 %copy-start.10 = (f32[512]{0:T(512)S(1)}, f32[512]{0:T(512)}, u32[]{:S(2)}) copy-start(f32[512]{0:T(512)} %param.22) | copy-start | bytes 6148
  0.0 3.0 %copy-start.9 = (f32[512]{0:T(512)S(1)}, f32[512]{0:T(512)}, u32[]{:S(2)}) copy-start(f32[512]{0:T(512)} %param.21) | copy-start | bytes 6148
  0.9 10.7 %collective-permute-start = (bf16[40,512]{1,0:T(8,128)(2,1)S(1)}, bf16[40,512]{1,0:T(8,128)(2,1)S(1)}, u32[]{:S(2)}, u32[]{:S(2)}) collective-permute-start(bf16[40,512]{1,0:T(8,128)(2,1)S(1)} %pack.1), channel_id=1, source_target_pairs={{0,2},{2,4},{4,6},{6,8},{8,10},{10,12},{12,14},{14,16},{16,18},{18... | collective-permute-start | bytes 122888 | tf_op jit(solution)/shard_map/ppermute | solution.py:21
  5.6 8.9 %copy-start.12 = (s32[128,2]{0,1:T(2,128)S(1)}, s32[128,2]{0,1:T(2,128)}, u32[]{:S(2)}) copy-start(s32[128,2]{0,1:T(2,128)} %param.26) | copy-start | bytes 3076
  5.6 8.8 %copy-start.13 = (f32[128,2]{0,1:T(2,128)S(1)}, f32[128,2]{0,1:T(2,128)}, u32[]{:S(2)}) copy-start(f32[128,2]{0,1:T(2,128)} %param.27) | copy-start | bytes 3076
  12.8 2.6 %collective-permute-start.1 = (bf16[128,512]{1,0:T(8,128)(2,1)S(1)}, bf16[128,512]{1,0:T(8,128)(2,1)S(1)}, u32[]{:S(2)}, u32[]{:S(2)}) collective-permute-start(bf16[128,512]{1,0:T(8,128)(2,1)S(1)} %get-tuple-element.13), channel_id=1, source_target_pairs={{0,1},{1,0},{2,3},{3,2},{4,5},{5,4},{6,7},{7,6},{8,9},{9,8},{10,11... | collective-permute-start | bytes 393224 | tf_op jit(solution)/shard_map/ppermute | solution.py:330
  14.5 2.2 %copy-start = (bf16[1024,2048]{1,0:T(8,128)(2,1)S(1)}, bf16[1024,2048]{1,0:T(8,128)(2,1)}, u32[]{:S(2)}) copy-start(bf16[1024,2048]{1,0:T(8,128)(2,1)} %conv_out.1) | copy-start | bytes 12582916
  14.5 2.3 %copy-start.4 = (bf16[128,2048]{1,0:T(8,128)(2,1)S(1)}, bf16[128,2048]{1,0:T(8,128)(2,1)}, u32[]{:S(2)}) copy-start(bf16[128,2048]{1,0:T(8,128)(2,1)} %residual.1) | copy-start | bytes 1572868
  14.5 2.3 %copy-start.8 = (f32[2048]{0:T(1024)S(1)}, f32[2048]{0:T(1024)}, u32[]{:S(2)}) copy-start(f32[2048]{0:T(1024)} %param.25) | copy-start | bytes 24580
  16.8 35.5 %copy-start.3 = (bf16[1,512,2048]{2,1,0:T(8,128)(2,1)S(1)}, bf16[1,512,2048]{2,1,0:T(8,128)(2,1)}, u32[]{:S(2)}) copy-start(bf16[1,512,2048]{2,1,0:T(8,128)(2,1)} %param.30) | copy-start | bytes 6291460
  18.6 33.7 %copy-start.1 = (bf16[1,2048,512]{2,1,0:T(8,128)(2,1)S(1)}, bf16[1,2048,512]{2,1,0:T(8,128)(2,1)}, u32[]{:S(2)}) copy-start(bf16[1,2048,512]{2,1,0:T(8,128)(2,1)} %param.28) | copy-start | bytes 6291460
  18.6 33.7 %copy-start.2 = (bf16[1,2048,512]{2,1,0:T(8,128)(2,1)S(1)}, bf16[1,2048,512]{2,1,0:T(8,128)(2,1)}, u32[]{:S(2)}) copy-start(bf16[1,2048,512]{2,1,0:T(8,128)(2,1)} %param.29) | copy-start | bytes 6291460
  57.7 35.0 %all-to-all-start.1 = ((bf16[128,8,1024]{2,1,0:T(8,128)(2,1)}), bf16[128,8,1024]{2,1,0:T(8,128)(2,1)S(1)}, u32[]{:S(2)}, u32[]{:S(2)}) async-start(bf16[128,8,1024]{2,1,0:T(8,128)(2,1)} %bitcast.29), calls=%async_computation.1 | async-start | bytes 4194304 | tf_op jit(solution)/shard_map/all_to_all | solution.py:382

commit v3 on v2

--- a/solution.py
+++ b/solution.py
@@ -100,9 +100,9 @@
         column, halo[HALO : HALO + 1, 0:128].astype(F32), 0, 128, width
     )
     at = pl.multiple_of(mine * tokens, tokens)
-    keep[...] = act[pl.ds(at, tokens), :]
+    keep[rows:, :] = act[pl.ds(at + rows, tokens - rows), :]
     at = pl.multiple_of((1 - mine) * tokens, tokens)
-    send[...] = act[pl.ds(at, tokens), :]
+    send[rows:, :] = act[pl.ds(at + rows, tokens - rows), :]
     ext[2 * HALO :, :] = jnp.zeros((8, 128), F32)
     for c in range(channels // 128):
         lanes = slice(c * 128, c * 128 + 128)
@@ -119,13 +119,9 @@
 
         first = normalized(fetch, deep, taps, gain, shift, lanes)
 
-        @pl.when(mine == 0)
-        def _():
-            keep[0:rows, lanes] = first
-
-        @pl.when(mine == 1)
-        def _():
-            send[0:rows, lanes] = first
+        second = act[tokens : tokens + rows, lanes]
+        keep[0:rows, lanes] = jnp.where(mine == 0, first, second)
+        send[0:rows, lanes] = jnp.where(mine == 0, second, first)
 
 
 def route_kernel(routes, weights, meta, pick):
@@ -170,27 +166,37 @@
     outgoing[...] = jnp.dot(pick[...], source, preferred_element_type=F32).astype(BF16)
 
 
-def expert_kernel(x, gate, up, down, out):
-    rows, half = out.shape
-    at = pl.ds(pl.multiple_of(pl.program_id(0) * rows, rows), rows)
-    quads = rows // 16
-    wide = x[at, :].astype(F32).reshape(quads, 2, 8, half)
-    a, b = wide[:, 0], wide[:, 1]
-    low = lax.broadcasted_iota(jnp.int32, (quads, 8, half), 1) < 4
-    top = jnp.where(low, a, pltpu.roll(b, 4, 1)).reshape(quads * 8, half).astype(BF16)
-    bottom = jnp.where(low, pltpu.roll(a, 4, 1), b).reshape(quads * 8, half).astype(BF16)
-
-    def apply(w):
-        return jnp.dot(top, w[0:half, :], preferred_element_type=F32) + jnp.dot(
-            bottom, w[half:, :], preferred_element_type=F32
-        )
-
-    hidden = (jax.nn.silu(apply(gate)) * apply(up)).astype(BF16)
-    left = jnp.dot(hidden, down[:, 0:half], preferred_element_type=F32).reshape(quads, 8, half)
-    right = jnp.dot(hidden, down[:, half:], preferred_element_type=F32).reshape(quads, 8, half)
-    first = jnp.where(low, left, pltpu.roll(right, 4, 1))
-    second = jnp.where(low, pltpu.roll(left, 4, 1), right)
-    out[...] = jnp.stack([first, second], axis=1).reshape(rows, half).astype(BF16)
+def expert_kernel(x, gate, up, down, out, rows, done, sems):
+    total, half = x.shape
+    quads = total // 16
+    piece = 256
+
+    def low(width):
+        return lax.broadcasted_iota(jnp.int32, (quads, 8, width), 1) < 4
+
+    for at in range(0, half, piece):
+        wide = x[:, at : at + piece].astype(F32).reshape(quads, 2, 8, piece)
+        a, b = wide[:, 0], wide[:, 1]
+        top = jnp.where(low(piece), a, pltpu.roll(b, 4, 1))
+        bottom = jnp.where(low(piece), pltpu.roll(a, 4, 1), b)
+        rows[:, at : at + piece] = top.reshape(quads * 8, piece).astype(BF16)
+        rows[:, half + at : half + at + piece] = bottom.reshape(quads * 8, piece).astype(BF16)
+    g = jnp.dot(rows[...], gate[...], preferred_element_type=F32)
+    u = jnp.dot(rows[...], up[...], preferred_element_type=F32)
+    hidden = (jax.nn.silu(g) * u).astype(BF16)
+    copies = []
+    for n, at in enumerate(range(0, half, piece)):
+        left = jnp.dot(hidden, down[:, at : at + piece], preferred_element_type=F32)
+        right = jnp.dot(hidden, down[:, half + at : half + at + piece], preferred_element_type=F32)
+        left = left.reshape(quads, 8, piece)
+        right = right.reshape(quads, 8, piece)
+        first = jnp.where(low(piece), left, pltpu.roll(right, 4, 1))
+        second = jnp.where(low(piece), pltpu.roll(left, 4, 1), right)
+        done[n] = jnp.stack([first, second], axis=1).reshape(total, piece).astype(BF16)
+        copies.append(pltpu.make_async_copy(done.at[n], out.at[:, at : at + piece], sems.at[n]))
+        copies[-1].start()
+    for copy in copies:
+        copy.wait()
 
 
 def shared_kernel(normed, stream, gate, up, down, out):
@@ -209,25 +215,33 @@
         out[...] += part
 
 
-def gather_kernel(returned, meta, base, out):
+def gather_kernel(returned, meta, base, out, ready, sems):
     rows, half = returned.shape
     tokens = base.shape[0]
-    h = pl.program_id(0)
+    piece = 256
     columns = jnp.transpose(meta[...])
     r = lax.broadcasted_iota(jnp.int32, (tokens, rows), 1)
     slots = ((r // 8) * 4 + r % 4).astype(F32)
-    here = (r // 4) % 2 == h
     weight = jnp.where(
-        here & (slots == columns[:, 0:1]),
+        slots == columns[:, 0:1],
         columns[:, 2:3],
-        jnp.where(here & (slots == columns[:, 1:2]), columns[:, 3:4], 0.0),
-    )
-    high = weight.astype(BF16)
-    low = (weight - high.astype(F32)).astype(BF16)
-    routed = jnp.dot(high, returned[...], preferred_element_type=F32) + jnp.dot(
-        low, returned[...], preferred_element_type=F32
-    )
-    out[...] = (base[:, pl.ds(pl.multiple_of(h * half, half), half)] + routed).astype(BF16)
+        jnp.where(slots == columns[:, 1:2], columns[:, 3:4], 0.0),
+    )
+    lower = (r // 4) % 2 == 0
+    weights = jnp.concatenate(
+        [jnp.where(lower, weight, 0.0), jnp.where(lower, 0.0, weight)], axis=0
+    ).astype(BF16)
+    copies = []
+    for n, at in enumerate(range(0, half, piece)):
+        routed = jnp.dot(weights, returned[:, at : at + piece], preferred_element_type=F32)
+        for h in range(2):
+            k = 2 * n + h
+            here = slice(h * half + at, h * half + at + piece)
+            ready[k] = (base[:, here] + routed[h * tokens : (h + 1) * tokens, :]).astype(BF16)
+            copies.append(pltpu.make_async_copy(ready.at[k], out.at[:, here], sems.at[k]))
+            copies[-1].start()
+    for copy in copies:
+        copy.wait()
 
 
 def whole(shape):
@@ -324,7 +338,7 @@
             held(shift),
         ],
         [((tokens, channels), BF16, None), ((tokens, channels), BF16, None)],
-        us=1,
+        us=0.3,
         scratch=[pltpu.VMEM((2 * HALO + 8, 128), F32), pltpu.VMEM((8, 2 * HALO, 128), F32)],
     )
     got = lax.ppermute(send, "tp", [(0, 1), (1, 0)])
@@ -333,7 +347,7 @@
         "route",
         [held(routes.T), held(route_weight.T)],
         [((8, tokens), F32, None), ((8 * experts, 2 * tokens), BF16, None)],
-        us=2,
+        us=0.3,
     )
     rows = (tokens, model_width)
     stream, normed, outgoing = kernel(
@@ -371,22 +385,30 @@
         us=8,
         grid=shared_gate.shape[1] // piece,
     )
+    outside = pl.BlockSpec(memory_space=pltpu.HBM)
     (result,) = kernel(
         expert_kernel,
         "expert",
         [held(arrived), held(expert_gate[0]), held(expert_up[0]), held(expert_down[0])],
-        [((8 * experts, half), BF16, pl.BlockSpec((2 * experts, half), lambda i: (i, 0)))],
+        [((8 * experts, half), BF16, outside)],
         us=5,
-        grid=4,
+        scratch=[
+            pltpu.VMEM((4 * experts, model_width), BF16),
+            pltpu.VMEM((half // 256, 8 * experts, 256), BF16),
+            pltpu.SemaphoreType.DMA((half // 256,)),
+        ],
     )
     returned = exchange(result.reshape(experts, 8, half)).reshape(8 * experts, half)
     (out,) = kernel(
         gather_kernel,
         "gather",
         [held(returned), held(meta), held(base)],
-        [(rows, BF16, pl.BlockSpec((tokens, half), lambda i: (0, i)))],
+        [(rows, BF16, outside)],
         us=2,
-        grid=2,
+        scratch=[
+            pltpu.VMEM((model_width // 256, tokens, 256), BF16),
+            pltpu.SemaphoreType.DMA((model_width // 256,)),
+        ],
     )
     return out
 

time: 95.5 us -> 91.9 us (0.962)
  Pallas kernels: 21 us -> 18.4 us
  local copies, waits for them, and re-layouts: 1.38 us -> 0.07 us
    pallas_call x8, Pallas kernels: 21 us -> 18.4 us  [kernel(): pl.pallas_call(body, grid=(grid,), in_specs=[spec for _, spec in args], o...]
    unnamed x28, local copies, waits for them, and re-layouts: 1.38 us -> 0.07 us
where the time goes in v3:
time: 91.9 us; the launch traced here: 91.7 us
  blocking collectives  34 us (37%)
  waiting for transfers between devices  30.9 us (34%)
  Pallas kernels  18.4 us (20%)
  starting transfers between devices  8.15 us (9%)
    all_to_all x1, blocking collectives, per_device(): exchange(outgoing.reshape(experts, 8, half)).reshape(8 * experts, half)  34 us
    all_to_all x1, waiting for transfers between devices, per_device(): exchange(result.reshape(experts, 8, half)).reshape(8 * experts, half)  24.8 us
    pallas_call x8, Pallas kernels, kernel(): pl.pallas_call(body, grid=(grid,), in_specs=[spec for _, spec in args], o...  18.4 us
    ppermute x1, waiting for transfers between devices, from_behind(): return lax.ppermute(x, axis, pairs)  5.89 us
    all_to_all x1, starting transfers between devices, per_device(): exchange(result.reshape(experts, 8, half)).reshape(8 * experts, half)  4.43 us
    ppermute x1, starting transfers between devices, from_behind(): return lax.ppermute(x, axis, pairs)  2.1 us
  transfers between devices with their start and end apart: 3, of which 3 were waited for; matrix products, arithmetic and copies ran while one was open for 0% of the time, Pallas kernels for 10%

profile of v3, /device:TPU:1, one launch (start us, length us, event | category | flops | bytes accessed | tf_op | source)
XLA Modules:
  0.0 91.7 jit_solution(18406544391840248189)
XLA Ops:
  0.0 0.0 copy-start.6
  0.0 0.0 copy-start.5
  0.0 0.0 copy-start.11
  0.0 0.0 copy-start.7
  0.0 0.0 copy-start.10
  0.0 0.0 copy-start.9
  0.0 0.8 pack.1
  0.9 2.1 %collective-permute-start = (bf16[40,512]{1,0:T(8,128)(2,1)S(1)}, bf16[40,512]{1,0:T(8,128)(2,1)S(1)}, u32[]{:S(2)}, u32[]{:S(2)}) collective-permute-start(bf16[40,512]{1,0:T(8,128)(2,1)S(1)} %pack.1), channel_id=1, source_target_pairs={{0,2},{2,4},{4,6},{6,8},{8,10},{10,12},{12,14},{14,16},{16,18},{18... | collective-permute-start | bytes 122888 | tf_op jit(solution)/shard_map/ppermute | solution.py:21
  3.0 0.0 copy-done.6
  3.0 0.0 copy-done.5
  3.0 0.0 copy-done.11
  3.0 0.0 copy-done.7
  3.0 0.0 copy-done.10
  3.0 0.0 copy-done.9
  3.0 0.0 copy-start.12
  3.0 0.0 copy-start.13
  3.0 0.0 copy-start
  3.1 2.6 %conv.1.act = bf16[256,512]{1,0:T(8,128)(2,1)S(1)} custom-call(bf16[256,512]{1,0:T(8,128)(2,1)S(1)} %copy-done.5, bf16[256,512]{1,0:T(8,128)(2,1)S(1)} %copy-done.6, bf16[31,512]{1,0:T(8,128)(2,1)S(1)} %copy-done.7, s32[1,256]{1,0:T(1,128)S(1)} %bitcast.25, f32[1,512]{1,0:T(1,128)S(1)} %bitcast.20, f32[1,512]{1,0:T(1,128)S(1)} %bitcast.22), custom_call_target="tpu_custom_call" | custom-call | flops 4000000000 | bytes 1000 | tf_op jit(solution)/shard_map/conv/pallas_call | solution.py:262
  5.7 0.0 copy-start.4
  5.7 0.0 copy-start.8
  5.7 5.9 %collective-permute-done.halo = bf16[40,512]{1,0:T(8,128)(2,1)S(1)} collective-permute-done((bf16[40,512]{1,0:T(8,128)(2,1)S(1)}, bf16[40,512]{1,0:T(8,128)(2,1)S(1)}, u32[]{:S(2)}, u32[]{:S(2)}) %collective-permute-start) | collective-permute-done | bytes 40992 | tf_op jit(solution)/shard_map/ppermute | solution.py:21
  11.6 0.7 rim.1
  12.2 1.6 %collective-permute-start.1 = (bf16[128,512]{1,0:T(8,128)(2,1)S(1)}, bf16[128,512]{1,0:T(8,128)(2,1)S(1)}, u32[]{:S(2)}, u32[]{:S(2)}) collective-permute-start(bf16[128,512]{1,0:T(8,128)(2,1)S(1)} %get-tuple-element.13), channel_id=1, source_target_pairs={{0,1},{1,0},{2,3},{3,2},{4,5},{5,4},{6,7},{7,6},{8,9},{9,8},{10,11... | collective-permute-start | bytes 393224 | tf_op jit(solution)/shard_map/ppermute | solution.py:344
  13.9 0.0 copy-done.12
  13.9 0.0 copy-done.13
  13.9 0.8 route.1
  14.7 0.2 collective-permute-done.1.got
  14.8 0.0 copy-done
  14.9 0.0 copy-done.4
  14.9 0.0 copy-done.8
  14.9 0.0 copy-start.3
  14.9 1.8 %spread.1 = (bf16[128,2048]{1,0:T(8,128)(2,1)}, bf16[128,2048]{1,0:T(8,128)(2,1)}, bf16[1024,1024]{1,0:T(8,128)(2,1)S(1)}) custom-call(bf16[128,512]{1,0:T(8,128)(2,1)S(1)} %get-tuple-element.12.keep, bf16[128,512]{1,0:T(8,128)(2,1)S(1)} %collective-permute-done.1.got, bf16[1024,2048]{1,0:T(8,128)(2,1)S(1)} %copy-done, bf16[128,2048]{1,0:T(8,128)(2,1)S(1)} %copy-done.4, ...), custom_call_target="tpu_custom_call" | custom-call | flops 3000000000 | bytes 1000 | tf_op jit(solution)/shard_map/spread/pallas_call | solution.py:262
  16.7 0.0 copy-start.1
  16.7 0.0 copy-start.2
  16.7 34.0 %all_to_all.10 = bf16[128,8,1024]{2,1,0:T(8,128)(2,1)S(1)} all-to-all(bf16[128,8,1024]{2,1,0:T(8,128)(2,1)S(1)} %bitcast.14), channel_id=1, replica_groups=mesh['sp'=64,'tp'=2] {'sp','tp'}, dimensions={0} | all-to-all | bytes 4194304 | tf_op jit(solution)/shard_map/all_to_all | solution.py:371
  50.7 0.0 copy-done.3
  50.7 0.0 copy-done.1
  50.7 0.0 copy-done.2
  50.7 4.3 %expert.1 = bf16[1024,1024]{1,0:T(8,128)(2,1)} custom-call(bf16[1024,1024]{1,0:T(8,128)(2,1)S(1)} %bitcast.15, bf16[2048,512]{1,0:T(8,128)(2,1)S(1)} %bitcast.16, bf16[2048,512]{1,0:T(8,128)(2,1)S(1)} %bitcast.17, bf16[512,2048]{1,0:T(8,128)(2,1)S(1)} %bitcast.18), custom_call_target="tpu_custom_call" | custom-call | flops 5000000000 | bytes 1000 | tf_op jit(solution)/shard_map/expert/pallas_call | solution.py:262
  55.0 4.4 %all-to-all-start.1 = ((bf16[128,8,1024]{2,1,0:T(8,128)(2,1)}), bf16[128,8,1024]{2,1,0:T(8,128)(2,1)S(1)}, u32[]{:S(2)}, u32[]{:S(2)}) async-start(bf16[128,8,1024]{2,1,0:T(8,128)(2,1)} %bitcast.29), calls=%async_computation.1 | async-start | bytes 4194304 | tf_op jit(solution)/shard_map/all_to_all | solution.py:401
  59.5 5.8 %shared.1.base = f32[128,2048]{1,0:T(8,128)S(1)} custom-call(bf16[128,2048]{1,0:T(8,128)(2,1)} %get-tuple-element.17.normed, bf16[128,2048]{1,0:T(8,128)(2,1)} %get-tuple-element.18.stream, bf16[2048,512]{1,0:T(8,128)(2,1)} %gate.7, bf16[2048,512]{1,0:T(8,128)(2,1)} %up.1, bf16[512,2048]{1,0:T(8,128)(2,1)} %down.1), custom_call_target="tpu_custom_call" | custom-call | flops 8000000000 | bytes 1000 | tf_op jit(solution)/shard_map/shared/pallas_call | solution.py:262
  65.2 24.8 %all-to-all-done.1 = bf16[128,8,1024]{2,1,0:T(8,128)(2,1)S(1)} async-done(((bf16[128,8,1024]{2,1,0:T(8,128)(2,1)}), bf16[128,8,1024]{2,1,0:T(8,128)(2,1)S(1)}, u32[]{:S(2)}, u32[]{:S(2)}) %all-to-all-start.1) | async-done | bytes 2097184 | tf_op jit(solution)/shard_map/all_to_all | solution.py:401
  90.1 1.6 %gather.1 = bf16[128,2048]{1,0:T(8,128)(2,1)} custom-call(bf16[1024,1024]{1,0:T(8,128)(2,1)S(1)} %bitcast.13, f32[8,128]{1,0:T(8,128)S(1)} %get-tuple-element.16.meta, f32[128,2048]{1,0:T(8,128)S(1)} %shared.1.base), custom_call_target="tpu_custom_call" | custom-call | flops 2000000000 | bytes 1000 | tf_op jit(solution)/shard_map/gather/pallas_call | solution.py:262
Async XLA Ops:
  0.0 3.0 %copy-start.6 = (bf16[256,512]{1,0:T(8,128)(2,1)S(1)}, bf16[256,512]{1,0:T(8,128)(2,1)}, u32[]{:S(2)}) copy-start(bf16[256,512]{1,0:T(8,128)(2,1)} %gate.6) | copy-start | bytes 786436
  0.0 3.0 %copy-start.5 = (bf16[256,512]{1,0:T(8,128)(2,1)S(1)}, bf16[256,512]{1,0:T(8,128)(2,1)}, u32[]{:S(2)}) copy-start(bf16[256,512]{1,0:T(8,128)(2,1)} %value.5) | copy-start | bytes 786436
  0.0 3.0 %copy-start.11 = (s32[256]{0:T(256)S(1)}, s32[256]{0:T(256)}, u32[]{:S(2)}) copy-start(s32[256]{0:T(256)} %param.20) | copy-start | bytes 3076
  0.0 3.0 %copy-start.7 = (bf16[31,512]{1,0:T(8,128)(2,1)S(1)}, bf16[31,512]{1,0:T(8,128)(2,1)}, u32[]{:S(2)}) copy-start(bf16[31,512]{1,0:T(8,128)(2,1)} %taps.3) | copy-start | bytes 95236
  0.0 3.0 %copy-start.10 = (f32[512]{0:T(512)S(1)}, f32[512]{0:T(512)}, u32[]{:S(2)}) copy-start(f32[512]{0:T(512)} %param.22) | copy-start | bytes 6148
  0.0 3.0 %copy-start.9 = (f32[512]{0:T(512)S(1)}, f32[512]{0:T(512)}, u32[]{:S(2)}) copy-start(f32[512]{0:T(512)} %param.21) | copy-start | bytes 6148
  0.9 10.7 %collective-permute-start = (bf16[40,512]{1,0:T(8,128)(2,1)S(1)}, bf16[40,512]{1,0:T(8,128)(2,1)S(1)}, u32[]{:S(2)}, u32[]{:S(2)}) collective-permute-start(bf16[40,512]{1,0:T(8,128)(2,1)S(1)} %pack.1), channel_id=1, source_target_pairs={{0,2},{2,4},{4,6},{6,8},{8,10},{10,12},{12,14},{14,16},{16,18},{18... | collective-permute-start | bytes 122888 | tf_op jit(solution)/shard_map/ppermute | solution.py:21
  3.0 10.8 %copy-start.12 = (s32[128,2]{0,1:T(2,128)S(1)}, s32[128,2]{0,1:T(2,128)}, u32[]{:S(2)}) copy-start(s32[128,2]{0,1:T(2,128)} %param.26) | copy-start | bytes 3076
  3.0 10.8 %copy-start.13 = (f32[128,2]{0,1:T(2,128)S(1)}, f32[128,2]{0,1:T(2,128)}, u32[]{:S(2)}) copy-start(f32[128,2]{0,1:T(2,128)} %param.27) | copy-start | bytes 3076
  3.0 11.8 %copy-start = (bf16[1024,2048]{1,0:T(8,128)(2,1)S(1)}, bf16[1024,2048]{1,0:T(8,128)(2,1)}, u32[]{:S(2)}) copy-start(bf16[1024,2048]{1,0:T(8,128)(2,1)} %conv_out.1) | copy-start | bytes 12582916
  5.7 9.2 %copy-start.4 = (bf16[128,2048]{1,0:T(8,128)(2,1)S(1)}, bf16[128,2048]{1,0:T(8,128)(2,1)}, u32[]{:S(2)}) copy-start(bf16[128,2048]{1,0:T(8,128)(2,1)} %residual.1) | copy-start | bytes 1572868
  5.7 9.2 %copy-start.8 = (f32[2048]{0:T(1024)S(1)}, f32[2048]{0:T(1024)}, u32[]{:S(2)}) copy-start(f32[2048]{0:T(1024)} %param.25) | copy-start | bytes 24580
  12.2 2.6 %collective-permute-start.1 = (bf16[128,512]{1,0:T(8,128)(2,1)S(1)}, bf16[128,512]{1,0:T(8,128)(2,1)S(1)}, u32[]{:S(2)}, u32[]{:S(2)}) collective-permute-start(bf16[128,512]{1,0:T(8,128)(2,1)S(1)} %get-tuple-element.13), channel_id=1, source_target_pairs={{0,1},{1,0},{2,3},{3,2},{4,5},{5,4},{6,7},{7,6},{8,9},{9,8},{10,11... | collective-permute-start | bytes 393224 | tf_op jit(solution)/shard_map/ppermute | solution.py:344
  14.9 35.8 %copy-start.3 = (bf16[1,512,2048]{2,1,0:T(8,128)(2,1)S(1)}, bf16[1,512,2048]{2,1,0:T(8,128)(2,1)}, u32[]{:S(2)}) copy-start(bf16[1,512,2048]{2,1,0:T(8,128)(2,1)} %param.30) | copy-start | bytes 6291460
  16.7 34.0 %copy-start.1 = (bf16[1,2048,512]{2,1,0:T(8,128)(2,1)S(1)}, bf16[1,2048,512]{2,1,0:T(8,128)(2,1)}, u32[]{:S(2)}) copy-start(bf16[1,2048,512]{2,1,0:T(8,128)(2,1)} %param.28) | copy-start | bytes 6291460
  16.7 34.0 %copy-start.2 = (bf16[1,2048,512]{2,1,0:T(8,128)(2,1)S(1)}, bf16[1,2048,512]{2,1,0:T(8,128)(2,1)}, u32[]{:S(2)}) copy-start(bf16[1,2048,512]{2,1,0:T(8,128)(2,1)} %param.29) | copy-start | bytes 6291460
  55.0 35.0 %all-to-all-start.1 = ((bf16[128,8,1024]{2,1,0:T(8,128)(2,1)}), bf16[128,8,1024]{2,1,0:T(8,128)(2,1)S(1)}, u32[]{:S(2)}, u32[]{:S(2)}) async-start(bf16[128,8,1024]{2,1,0:T(8,128)(2,1)} %bitcast.29), calls=%async_computation.1 | async-start | bytes 4194304 | tf_op jit(solution)/shard_map/all_to_all | solution.py:401

commit v4 on v3

--- a/solution.py
+++ b/solution.py
@@ -12,7 +12,6 @@
 F32 = jnp.float32
 BF16 = jnp.bfloat16
 HALO = 32
-PACK = 40
 
 
 def from_behind(x, axis, by):
@@ -29,10 +28,11 @@
 def pack_kernel(value, gate, ids, out):
     channels = value.shape[1]
     positions = ids.shape[1]
-    out[0:HALO, :] = glu_of(value[...], gate[...])
     tail = ids[:, positions - 128 :].astype(F32)
     row = jnp.concatenate([tail, jnp.zeros((1, channels - 128), F32)], axis=1)
-    out[HALO:, :] = jnp.broadcast_to(row, (PACK - HALO, channels)).astype(BF16)
+    first = lax.broadcasted_iota(jnp.int32, (HALO, channels), 0) == 0
+    rows = glu_of(value[...], gate[...]).astype(F32)
+    out[...] = jnp.where(first, row, rows).astype(BF16)
 
 
 def same_document(column, row, first, behind, width):
@@ -97,7 +97,7 @@
     own = ids[...].astype(F32)
     column = column_of(own)[0:rows]
     deep = same_document(column, own, 0, 0, width) + same_document(
-        column, halo[HALO : HALO + 1, 0:128].astype(F32), 0, 128, width
+        column, halo[0:1, 0:128].astype(F32), 0, 128, width
     )
     at = pl.multiple_of(mine * tokens, tokens)
     keep[rows:, :] = act[pl.ds(at + rows, tokens - rows), :]
@@ -147,23 +147,29 @@
         pick[:, h * tokens : (h + 1) * tokens] = (chosen & (half == h)).astype(F32).astype(BF16)
 
 
-def spread_kernel(keep, got, conv_out, residual, norm_gain, pick, stream, normed, outgoing):
+def spread_kernel(keep, got, conv_out, residual, norm_gain, pick, stream, normed, outgoing, left, right, sems):
     tokens, half_in = keep.shape
     model_width = residual.shape[1]
     mine = lax.axis_index("tp")
-    first = pl.multiple_of(mine * half_in, half_in)
+    near = pl.multiple_of(mine * half_in, half_in)
     other = pl.multiple_of((1 - mine) * half_in, half_in)
-    part = jnp.dot(keep[...], conv_out[pl.ds(first, half_in), :], preferred_element_type=F32)
+    part = jnp.dot(keep[...], conv_out[pl.ds(near, half_in), :], preferred_element_type=F32)
     part = part + jnp.dot(got[...], conv_out[pl.ds(other, half_in), :], preferred_element_type=F32)
     rows = (residual[...].astype(F32) + part).astype(BF16)
-    stream[...] = rows
+    left[...] = rows
+    first = pltpu.make_async_copy(left, stream, sems.at[0])
+    first.start()
     wide = rows.astype(F32)
     scale = lax.rsqrt(jnp.mean(wide * wide, axis=-1, keepdims=True) + EPS)
     ready = (wide * scale * norm_gain[...]).astype(BF16)
-    normed[...] = ready
+    right[...] = ready
+    second = pltpu.make_async_copy(right, normed, sems.at[1])
+    second.start()
     mid = model_width // 2
     source = jnp.concatenate([ready[:, 0:mid], ready[:, mid:]], axis=0)
     outgoing[...] = jnp.dot(pick[...], source, preferred_element_type=F32).astype(BF16)
+    first.wait()
+    second.wait()
 
 
 def expert_kernel(x, gate, up, down, out, rows, done, sems):
@@ -308,7 +314,7 @@
         pack_kernel,
         "pack",
         [copied(conv_value, tail), copied(conv_gate, tail), copied(ids)],
-        [((PACK, channels), BF16, None)],
+        [((HALO, channels), BF16, None)],
         us=1,
     )
     halo = from_behind(packed, "sp", 1)
@@ -350,6 +356,7 @@
         us=0.3,
     )
     rows = (tokens, model_width)
+    outside = pl.BlockSpec(memory_space=pltpu.HBM)
     stream, normed, outgoing = kernel(
         spread_kernel,
         "spread",
@@ -361,8 +368,9 @@
             held(norm_gain.reshape(1, model_width)),
             held(pick),
         ],
-        [(rows, BF16, whole(rows)), (rows, BF16, whole(rows)), ((8 * experts, half), BF16, None)],
+        [(rows, BF16, outside), (rows, BF16, outside), ((8 * experts, half), BF16, None)],
         us=3,
+        scratch=[pltpu.VMEM(rows, BF16), pltpu.VMEM(rows, BF16), pltpu.SemaphoreType.DMA((2,))],
     )
 
     exchange = functools.partial(
@@ -385,7 +393,6 @@
         us=8,
         grid=shared_gate.shape[1] // piece,
     )
-    outside = pl.BlockSpec(memory_space=pltpu.HBM)
     (result,) = kernel(
         expert_kernel,
         "expert",

time: 91.9 us -> 91.9 us (level)
  no operation moved by 1% of the time
where the time goes in v4:
time: 91.9 us; the launch traced here: 91.7 us
  blocking collectives  34 us (37%)
  waiting for transfers between devices  30.9 us (34%)
  Pallas kernels  18.4 us (20%)
  starting transfers between devices  8.14 us (9%)
    all_to_all x1, blocking collectives, per_device(): exchange(outgoing.reshape(experts, 8, half)).reshape(8 * experts, half)  34 us
    all_to_all x1, waiting for transfers between devices, per_device(): exchange(result.reshape(experts, 8, half)).reshape(8 * experts, half)  24.8 us
    pallas_call x8, Pallas kernels, kernel(): pl.pallas_call(body, grid=(grid,), in_specs=[spec for _, spec in args], o...  18.4 us
    ppermute x1, waiting for transfers between devices, from_behind(): return lax.ppermute(x, axis, pairs)  5.83 us
    all_to_all x1, starting transfers between devices, per_device(): exchange(result.reshape(experts, 8, half)).reshape(8 * experts, half)  4.42 us
    ppermute x1, starting transfers between devices, from_behind(): return lax.ppermute(x, axis, pairs)  2.1 us
  transfers between devices with their start and end apart: 3, of which 3 were waited for; matrix products, arithmetic and copies ran while one was open for 0% of the time, Pallas kernels for 10%

profile of v4, /device:TPU:1, one launch (start us, length us, event | category | flops | bytes accessed | tf_op | source)
XLA Modules:
  0.0 91.7 jit_solution(9795861637855931184)
XLA Ops:
  0.0 0.0 copy-start.6
  0.0 0.0 copy-start.5
  0.0 0.0 copy-start.11
  0.0 0.0 copy-start.7
  0.0 0.0 copy-start.10
  0.0 0.0 copy-start.9
  0.0 0.8 pack.1
  0.9 2.1 %collective-permute-start = (bf16[32,512]{1,0:T(8,128)(2,1)S(1)}, bf16[32,512]{1,0:T(8,128)(2,1)S(1)}, u32[]{:S(2)}, u32[]{:S(2)}) collective-permute-start(bf16[32,512]{1,0:T(8,128)(2,1)S(1)} %pack.1), channel_id=1, source_target_pairs={{0,2},{2,4},{4,6},{6,8},{8,10},{10,12},{12,14},{14,16},{16,18},{18... | collective-permute-start | bytes 98312 | tf_op jit(solution)/shard_map/ppermute | solution.py:20
  3.0 0.0 copy-done.6
  3.0 0.0 copy-done.5
  3.0 0.0 copy-done.11
  3.0 0.0 copy-done.7
  3.0 0.0 copy-done.10
  3.0 0.0 copy-done.9
  3.0 0.0 copy-start.12
  3.0 0.0 copy-start.13
  3.0 0.0 copy-start
  3.1 2.6 %conv.1.act = bf16[256,512]{1,0:T(8,128)(2,1)S(1)} custom-call(bf16[256,512]{1,0:T(8,128)(2,1)S(1)} %copy-done.5, bf16[256,512]{1,0:T(8,128)(2,1)S(1)} %copy-done.6, bf16[31,512]{1,0:T(8,128)(2,1)S(1)} %copy-done.7, s32[1,256]{1,0:T(1,128)S(1)} %bitcast.25, f32[1,512]{1,0:T(1,128)S(1)} %bitcast.20, f32[1,512]{1,0:T(1,128)S(1)} %bitcast.22), custom_call_target="tpu_custom_call" | custom-call | flops 4000000000 | bytes 1000 | tf_op jit(solution)/shard_map/conv/pallas_call | solution.py:268
  5.6 0.0 copy-start.4
  5.6 0.0 copy-start.8
  5.7 5.8 %collective-permute-done.halo = bf16[32,512]{1,0:T(8,128)(2,1)S(1)} collective-permute-done((bf16[32,512]{1,0:T(8,128)(2,1)S(1)}, bf16[32,512]{1,0:T(8,128)(2,1)S(1)}, u32[]{:S(2)}, u32[]{:S(2)}) %collective-permute-start) | collective-permute-done | bytes 32800 | tf_op jit(solution)/shard_map/ppermute | solution.py:20
  11.5 0.7 rim.1
  12.1 1.6 %collective-permute-start.1 = (bf16[128,512]{1,0:T(8,128)(2,1)S(1)}, bf16[128,512]{1,0:T(8,128)(2,1)S(1)}, u32[]{:S(2)}, u32[]{:S(2)}) collective-permute-start(bf16[128,512]{1,0:T(8,128)(2,1)S(1)} %get-tuple-element.13), channel_id=1, source_target_pairs={{0,1},{1,0},{2,3},{3,2},{4,5},{5,4},{6,7},{7,6},{8,9},{9,8},{10,11... | collective-permute-start | bytes 393224 | tf_op jit(solution)/shard_map/ppermute | solution.py:350
  13.8 0.0 copy-done.12
  13.8 0.0 copy-done.13
  13.8 0.8 route.1
  14.6 0.2 collective-permute-done.1.got
  14.8 0.0 copy-done
  14.8 0.0 copy-done.4
  14.8 0.0 copy-done.8
  14.8 0.0 copy-start.3
  14.8 1.8 %spread.1 = (bf16[128,2048]{1,0:T(8,128)(2,1)}, bf16[128,2048]{1,0:T(8,128)(2,1)}, bf16[1024,1024]{1,0:T(8,128)(2,1)S(1)}) custom-call(bf16[128,512]{1,0:T(8,128)(2,1)S(1)} %get-tuple-element.12.keep, bf16[128,512]{1,0:T(8,128)(2,1)S(1)} %collective-permute-done.1.got, bf16[1024,2048]{1,0:T(8,128)(2,1)S(1)} %copy-done, bf16[128,2048]{1,0:T(8,128)(2,1)S(1)} %copy-done.4, ...), custom_call_target="tpu_custom_call" | custom-call | flops 3000000000 | bytes 1000 | tf_op jit(solution)/shard_map/spread/pallas_call | solution.py:268
  16.6 0.0 copy-start.1
  16.6 0.0 copy-start.2
  16.6 34.0 %all_to_all.10 = bf16[128,8,1024]{2,1,0:T(8,128)(2,1)S(1)} all-to-all(bf16[128,8,1024]{2,1,0:T(8,128)(2,1)S(1)} %bitcast.14), channel_id=1, replica_groups=mesh['sp'=64,'tp'=2] {'sp','tp'}, dimensions={0} | all-to-all | bytes 4194304 | tf_op jit(solution)/shard_map/all_to_all | solution.py:379
  50.7 0.0 copy-done.3
  50.7 0.0 copy-done.1
  50.7 0.0 copy-done.2
  50.7 4.3 %expert.1 = bf16[1024,1024]{1,0:T(8,128)(2,1)} custom-call(bf16[1024,1024]{1,0:T(8,128)(2,1)S(1)} %bitcast.15, bf16[2048,512]{1,0:T(8,128)(2,1)S(1)} %bitcast.16, bf16[2048,512]{1,0:T(8,128)(2,1)S(1)} %bitcast.17, bf16[512,2048]{1,0:T(8,128)(2,1)S(1)} %bitcast.18), custom_call_target="tpu_custom_call" | custom-call | flops 5000000000 | bytes 1000 | tf_op jit(solution)/shard_map/expert/pallas_call | solution.py:268
  55.0 4.4 %all-to-all-start.1 = ((bf16[128,8,1024]{2,1,0:T(8,128)(2,1)}), bf16[128,8,1024]{2,1,0:T(8,128)(2,1)S(1)}, u32[]{:S(2)}, u32[]{:S(2)}) async-start(bf16[128,8,1024]{2,1,0:T(8,128)(2,1)} %bitcast.29), calls=%async_computation.1 | async-start | bytes 4194304 | tf_op jit(solution)/shard_map/all_to_all | solution.py:408
  59.4 5.8 %shared.1.base = f32[128,2048]{1,0:T(8,128)S(1)} custom-call(bf16[128,2048]{1,0:T(8,128)(2,1)} %get-tuple-element.17.normed, bf16[128,2048]{1,0:T(8,128)(2,1)} %get-tuple-element.18.stream, bf16[2048,512]{1,0:T(8,128)(2,1)} %gate.7, bf16[2048,512]{1,0:T(8,128)(2,1)} %up.1, bf16[512,2048]{1,0:T(8,128)(2,1)} %down.1), custom_call_target="tpu_custom_call" | custom-call | flops 8000000000 | bytes 1000 | tf_op jit(solution)/shard_map/shared/pallas_call | solution.py:268
  65.2 24.8 %all-to-all-done.1 = bf16[128,8,1024]{2,1,0:T(8,128)(2,1)S(1)} async-done(((bf16[128,8,1024]{2,1,0:T(8,128)(2,1)}), bf16[128,8,1024]{2,1,0:T(8,128)(2,1)S(1)}, u32[]{:S(2)}, u32[]{:S(2)}) %all-to-all-start.1) | async-done | bytes 2097184 | tf_op jit(solution)/shard_map/all_to_all | solution.py:408
  90.0 1.6 %gather.1 = bf16[128,2048]{1,0:T(8,128)(2,1)} custom-call(bf16[1024,1024]{1,0:T(8,128)(2,1)S(1)} %bitcast.13, f32[8,128]{1,0:T(8,128)S(1)} %get-tuple-element.16.meta, f32[128,2048]{1,0:T(8,128)S(1)} %shared.1.base), custom_call_target="tpu_custom_call" | custom-call | flops 2000000000 | bytes 1000 | tf_op jit(solution)/shard_map/gather/pallas_call | solution.py:268
Async XLA Ops:
  0.0 3.0 %copy-start.6 = (bf16[256,512]{1,0:T(8,128)(2,1)S(1)}, bf16[256,512]{1,0:T(8,128)(2,1)}, u32[]{:S(2)}) copy-start(bf16[256,512]{1,0:T(8,128)(2,1)} %gate.6) | copy-start | bytes 786436
  0.0 3.0 %copy-start.5 = (bf16[256,512]{1,0:T(8,128)(2,1)S(1)}, bf16[256,512]{1,0:T(8,128)(2,1)}, u32[]{:S(2)}) copy-start(bf16[256,512]{1,0:T(8,128)(2,1)} %value.5) | copy-start | bytes 786436
  0.0 3.0 %copy-start.11 = (s32[256]{0:T(256)S(1)}, s32[256]{0:T(256)}, u32[]{:S(2)}) copy-start(s32[256]{0:T(256)} %param.20) | copy-start | bytes 3076
  0.0 3.0 %copy-start.7 = (bf16[31,512]{1,0:T(8,128)(2,1)S(1)}, bf16[31,512]{1,0:T(8,128)(2,1)}, u32[]{:S(2)}) copy-start(bf16[31,512]{1,0:T(8,128)(2,1)} %taps.3) | copy-start | bytes 95236
  0.0 3.0 %copy-start.10 = (f32[512]{0:T(512)S(1)}, f32[512]{0:T(512)}, u32[]{:S(2)}) copy-start(f32[512]{0:T(512)} %param.22) | copy-start | bytes 6148
  0.0 3.0 %copy-start.9 = (f32[512]{0:T(512)S(1)}, f32[512]{0:T(512)}, u32[]{:S(2)}) copy-start(f32[512]{0:T(512)} %param.21) | copy-start | bytes 6148
  0.9 10.6 %collective-permute-start = (bf16[32,512]{1,0:T(8,128)(2,1)S(1)}, bf16[32,512]{1,0:T(8,128)(2,1)S(1)}, u32[]{:S(2)}, u32[]{:S(2)}) collective-permute-start(bf16[32,512]{1,0:T(8,128)(2,1)S(1)} %pack.1), channel_id=1, source_target_pairs={{0,2},{2,4},{4,6},{6,8},{8,10},{10,12},{12,14},{14,16},{16,18},{18... | collective-permute-start | bytes 98312 | tf_op jit(solution)/shard_map/ppermute | solution.py:20
  3.0 10.8 %copy-start.12 = (s32[128,2]{0,1:T(2,128)S(1)}, s32[128,2]{0,1:T(2,128)}, u32[]{:S(2)}) copy-start(s32[128,2]{0,1:T(2,128)} %param.26) | copy-start | bytes 3076
  3.0 10.7 %copy-start.13 = (f32[128,2]{0,1:T(2,128)S(1)}, f32[128,2]{0,1:T(2,128)}, u32[]{:S(2)}) copy-start(f32[128,2]{0,1:T(2,128)} %param.27) | copy-start | bytes 3076
  3.0 11.7 %copy-start = (bf16[1024,2048]{1,0:T(8,128)(2,1)S(1)}, bf16[1024,2048]{1,0:T(8,128)(2,1)}, u32[]{:S(2)}) copy-start(bf16[1024,2048]{1,0:T(8,128)(2,1)} %conv_out.1) | copy-start | bytes 12582916
  5.6 9.1 %copy-start.4 = (bf16[128,2048]{1,0:T(8,128)(2,1)S(1)}, bf16[128,2048]{1,0:T(8,128)(2,1)}, u32[]{:S(2)}) copy-start(bf16[128,2048]{1,0:T(8,128)(2,1)} %residual.1) | copy-start | bytes 1572868
  5.6 9.1 %copy-start.8 = (f32[2048]{0:T(1024)S(1)}, f32[2048]{0:T(1024)}, u32[]{:S(2)}) copy-start(f32[2048]{0:T(1024)} %param.25) | copy-start | bytes 24580
  12.1 2.6 %collective-permute-start.1 = (bf16[128,512]{1,0:T(8,128)(2,1)S(1)}, bf16[128,512]{1,0:T(8,128)(2,1)S(1)}, u32[]{:S(2)}, u32[]{:S(2)}) collective-permute-start(bf16[128,512]{1,0:T(8,128)(2,1)S(1)} %get-tuple-element.13), channel_id=1, source_target_pairs={{0,1},{1,0},{2,3},{3,2},{4,5},{5,4},{6,7},{7,6},{8,9},{9,8},{10,11... | collective-permute-start | bytes 393224 | tf_op jit(solution)/shard_map/ppermute | solution.py:350
  14.8 35.9 %copy-start.3 = (bf16[1,512,2048]{2,1,0:T(8,128)(2,1)S(1)}, bf16[1,512,2048]{2,1,0:T(8,128)(2,1)}, u32[]{:S(2)}) copy-start(bf16[1,512,2048]{2,1,0:T(8,128)(2,1)} %param.30) | copy-start | bytes 6291460
  16.6 34.1 %copy-start.1 = (bf16[1,2048,512]{2,1,0:T(8,128)(2,1)S(1)}, bf16[1,2048,512]{2,1,0:T(8,128)(2,1)}, u32[]{:S(2)}) copy-start(bf16[1,2048,512]{2,1,0:T(8,128)(2,1)} %param.28) | copy-start | bytes 6291460
  16.6 34.0 %copy-start.2 = (bf16[1,2048,512]{2,1,0:T(8,128)(2,1)S(1)}, bf16[1,2048,512]{2,1,0:T(8,128)(2,1)}, u32[]{:S(2)}) copy-start(bf16[1,2048,512]{2,1,0:T(8,128)(2,1)} %param.29) | copy-start | bytes 6291460
  55.0 35.0 %all-to-all-start.1 = ((bf16[128,8,1024]{2,1,0:T(8,128)(2,1)}), bf16[128,8,1024]{2,1,0:T(8,128)(2,1)S(1)}, u32[]{:S(2)}, u32[]{:S(2)}) async-start(bf16[128,8,1024]{2,1,0:T(8,128)(2,1)} %bitcast.29), calls=%async_computation.1 | async-start | bytes 4194304 | tf_op jit(solution)/shard_map/all_to_all | solution.py:408

commit v5 on v4

--- a/solution.py
+++ b/solution.py
@@ -124,7 +124,12 @@
         send[0:rows, lanes] = jnp.where(mine == 0, second, first)
 
 
-def route_kernel(routes, weights, meta, pick):
+def route_kernel(routes, weights, keep, conv_out, residual, meta, pick, part):
+    half_in = keep.shape[1]
+    near = pl.multiple_of(lax.axis_index("tp") * half_in, half_in)
+    part[...] = residual[...].astype(F32) + jnp.dot(
+        keep[...], conv_out[pl.ds(near, half_in), :], preferred_element_type=F32
+    )
     tokens = routes.shape[1]
     experts = pick.shape[0] // 8
     expert = lax.broadcasted_iota(jnp.int32, (experts, tokens), 0)
@@ -147,15 +152,12 @@
         pick[:, h * tokens : (h + 1) * tokens] = (chosen & (half == h)).astype(F32).astype(BF16)
 
 
-def spread_kernel(keep, got, conv_out, residual, norm_gain, pick, stream, normed, outgoing, left, right, sems):
-    tokens, half_in = keep.shape
-    model_width = residual.shape[1]
-    mine = lax.axis_index("tp")
-    near = pl.multiple_of(mine * half_in, half_in)
-    other = pl.multiple_of((1 - mine) * half_in, half_in)
-    part = jnp.dot(keep[...], conv_out[pl.ds(near, half_in), :], preferred_element_type=F32)
-    part = part + jnp.dot(got[...], conv_out[pl.ds(other, half_in), :], preferred_element_type=F32)
-    rows = (residual[...].astype(F32) + part).astype(BF16)
+def spread_kernel(got, conv_out, part, norm_gain, pick, stream, normed, outgoing, left, right, sems):
+    half_in = got.shape[1]
+    model_width = part.shape[1]
+    other = pl.multiple_of((1 - lax.axis_index("tp")) * half_in, half_in)
+    rows = jnp.dot(got[...], conv_out[pl.ds(other, half_in), :], preferred_element_type=F32)
+    rows = (part[...] + rows).astype(BF16)
     left[...] = rows
     first = pltpu.make_async_copy(left, stream, sems.at[0])
     first.start()
@@ -348,23 +350,22 @@
         scratch=[pltpu.VMEM((2 * HALO + 8, 128), F32), pltpu.VMEM((8, 2 * HALO, 128), F32)],
     )
     got = lax.ppermute(send, "tp", [(0, 1), (1, 0)])
-    meta, pick = kernel(
+    rows = (tokens, model_width)
+    outside = pl.BlockSpec(memory_space=pltpu.HBM)
+    meta, pick, part = kernel(
         route_kernel,
         "route",
-        [held(routes.T), held(route_weight.T)],
-        [((8, tokens), F32, None), ((8 * experts, 2 * tokens), BF16, None)],
+        [held(routes.T), held(route_weight.T), held(keep), held(conv_out), held(residual)],
+        [((8, tokens), F32, None), ((8 * experts, 2 * tokens), BF16, None), (rows, F32, None)],
         us=0.3,
     )
-    rows = (tokens, model_width)
-    outside = pl.BlockSpec(memory_space=pltpu.HBM)
     stream, normed, outgoing = kernel(
         spread_kernel,
         "spread",
         [
-            held(keep),
             held(got),
             held(conv_out),
-            held(residual),
+            held(part),
             held(norm_gain.reshape(1, model_width)),
             held(pick),
         ],

time: 91.9 us -> 91.6 us (level)
  transfers between devices with their start and end apart: 3 -> 3, of which waited for: 3 -> 2; matrix products, arithmetic and copies ran while one was open for 0% -> 0% of each run, Pallas kernels for 10% -> 10%
where the time goes in v5:
time: 91.6 us; the launch traced here: 91.4 us
  blocking collectives  33.8 us (37%)
  waiting for transfers between devices  30.7 us (34%)
  Pallas kernels  18.5 us (20%)
  starting transfers between devices  8.14 us (9%)
    all_to_all x1, blocking collectives, per_device(): exchange(outgoing.reshape(experts, 8, half)).reshape(8 * experts, half)  33.8 us
    all_to_all x1, waiting for transfers between devices, per_device(): exchange(result.reshape(experts, 8, half)).reshape(8 * experts, half)  24.8 us
    pallas_call x8, Pallas kernels, kernel(): pl.pallas_call(body, grid=(grid,), in_specs=[spec for _, spec in args], o...  18.5 us
    ppermute x1, waiting for transfers between devices, from_behind(): return lax.ppermute(x, axis, pairs)  5.84 us
    all_to_all x1, starting transfers between devices, per_device(): exchange(result.reshape(experts, 8, half)).reshape(8 * experts, half)  4.42 us
    ppermute x1, starting transfers between devices, from_behind(): return lax.ppermute(x, axis, pairs)  2.1 us
  transfers between devices with their start and end apart: 3, of which 2 were waited for; matrix products, arithmetic and copies ran while one was open for 0% of the time, Pallas kernels for 10%

profile of v5, /device:TPU:1, one launch (start us, length us, event | category | flops | bytes accessed | tf_op | source)
XLA Modules:
  0.0 91.4 jit_solution(2023615398442646577)
XLA Ops:
  0.0 0.0 copy-start.8
  0.0 0.0 copy-start.7
  0.0 0.0 copy-start.13
  0.0 0.0 copy-start.9
  0.0 0.0 copy-start.12
  0.0 0.0 copy-start.11
  0.0 0.8 pack.1
  0.9 2.1 %collective-permute-start = (bf16[32,512]{1,0:T(8,128)(2,1)S(1)}, bf16[32,512]{1,0:T(8,128)(2,1)S(1)}, u32[]{:S(2)}, u32[]{:S(2)}) collective-permute-start(bf16[32,512]{1,0:T(8,128)(2,1)S(1)} %pack.1), channel_id=1, source_target_pairs={{0,2},{2,4},{4,6},{6,8},{8,10},{10,12},{12,14},{14,16},{16,18},{18... | collective-permute-start | bytes 98312 | tf_op jit(solution)/shard_map/ppermute | solution.py:20
  3.0 0.0 copy-done.8
  3.0 0.0 copy-done.7
  3.0 0.0 copy-done.13
  3.0 0.0 copy-done.9
  3.0 0.0 copy-done.12
  3.0 0.0 copy-done.11
  3.0 0.0 copy-start
  3.0 0.0 copy-start.1
  3.0 0.0 copy-start.2
  3.1 0.0 copy-start.3
  3.1 2.6 %conv.1.act = bf16[256,512]{1,0:T(8,128)(2,1)S(1)} custom-call(bf16[256,512]{1,0:T(8,128)(2,1)S(1)} %copy-done.7, bf16[256,512]{1,0:T(8,128)(2,1)S(1)} %copy-done.8, bf16[31,512]{1,0:T(8,128)(2,1)S(1)} %copy-done.9, s32[1,256]{1,0:T(1,128)S(1)} %bitcast.27, f32[1,512]{1,0:T(1,128)S(1)} %bitcast.22, f32[1,512]{1,0:T(1,128)S(1)} %bitcast.24), custom_call_target="tpu_custom_call" | custom-call | flops 4000000000 | bytes 1000 | tf_op jit(solution)/shard_map/conv/pallas_call | solution.py:270
  5.6 5.8 %collective-permute-done.halo = bf16[32,512]{1,0:T(8,128)(2,1)S(1)} collective-permute-done((bf16[32,512]{1,0:T(8,128)(2,1)S(1)}, bf16[32,512]{1,0:T(8,128)(2,1)S(1)}, u32[]{:S(2)}, u32[]{:S(2)}) %collective-permute-start) | collective-permute-done | bytes 32800 | tf_op jit(solution)/shard_map/ppermute | solution.py:20
  11.5 0.7 rim.1
  12.1 1.6 %collective-permute-start.1 = (bf16[128,512]{1,0:T(8,128)(2,1)S(1)}, bf16[128,512]{1,0:T(8,128)(2,1)S(1)}, u32[]{:S(2)}, u32[]{:S(2)}) collective-permute-start(bf16[128,512]{1,0:T(8,128)(2,1)S(1)} %get-tuple-element.13), channel_id=1, source_target_pairs={{0,1},{1,0},{2,3},{3,2},{4,5},{5,4},{6,7},{7,6},{8,9},{9,8},{10,11... | collective-permute-start | bytes 393224 | tf_op jit(solution)/shard_map/ppermute | solution.py:352
  13.8 0.0 copy-done
  13.8 0.0 copy-done.1
  13.8 0.0 copy-done.2
  13.8 0.0 copy-done.3
  13.8 0.0 copy-start.10
  13.8 1.1 %route.1 = (f32[8,128]{1,0:T(8,128)S(1)}, bf16[1024,256]{1,0:T(8,128)(2,1)S(1)}, f32[128,2048]{1,0:T(8,128)S(1)}) custom-call(s32[2,128]{1,0:T(2,128)S(1)} %bitcast.16, f32[2,128]{1,0:T(2,128)S(1)} %bitcast.17, bf16[128,512]{1,0:T(8,128)(2,1)S(1)} %get-tuple-element.14.keep, bf16[1024,2048]{1,0:T(8,128)(2,1)S(1)} %copy-done, bf16[128,2048]{1,0:T(8,128)(2,1)S(1)} %copy-done.1), custom_call_target="tpu_custom_call" | custom-call | flops 300000000 | bytes 1000 | tf_op jit(solution)/shard_map/route/pallas_call | solution.py:270
  14.9 0.0 collective-permute-done.1.got
  14.9 0.0 copy-done.10
  14.9 0.0 copy-start.6
  15.0 1.6 %spread.1 = (bf16[128,2048]{1,0:T(8,128)(2,1)}, bf16[128,2048]{1,0:T(8,128)(2,1)}, bf16[1024,1024]{1,0:T(8,128)(2,1)S(1)}) custom-call(bf16[128,512]{1,0:T(8,128)(2,1)S(1)} %collective-permute-done.1.got, bf16[1024,2048]{1,0:T(8,128)(2,1)S(1)} %copy-done, f32[128,2048]{1,0:T(8,128)S(1)} %get-tuple-element.15.part, f32[1,2048]{1,0:T(1,128)S(1)} %bitcast.21, ...), custom_call_target="tpu_custom_call" | custom-call | flops 3000000000 | bytes 1000 | tf_op jit(solution)/shard_map/spread/pallas_call | solution.py:270
  16.5 0.0 copy-start.4
  16.5 0.0 copy-start.5
  16.5 33.8 %all_to_all.10 = bf16[128,8,1024]{2,1,0:T(8,128)(2,1)S(1)} all-to-all(bf16[128,8,1024]{2,1,0:T(8,128)(2,1)S(1)} %bitcast.14), channel_id=1, replica_groups=mesh['sp'=64,'tp'=2] {'sp','tp'}, dimensions={0} | all-to-all | bytes 4194304 | tf_op jit(solution)/shard_map/all_to_all | solution.py:380
  50.4 0.0 copy-done.6
  50.4 0.0 copy-done.4
  50.4 0.0 copy-done.5
  50.4 4.4 %expert.1 = bf16[1024,1024]{1,0:T(8,128)(2,1)} custom-call(bf16[1024,1024]{1,0:T(8,128)(2,1)S(1)} %bitcast.15, bf16[2048,512]{1,0:T(8,128)(2,1)S(1)} %bitcast.18, bf16[2048,512]{1,0:T(8,128)(2,1)S(1)} %bitcast.19, bf16[512,2048]{1,0:T(8,128)(2,1)S(1)} %bitcast.20), custom_call_target="tpu_custom_call" | custom-call | flops 5000000000 | bytes 1000 | tf_op jit(solution)/shard_map/expert/pallas_call | solution.py:270
  54.8 4.4 %all-to-all-start.1 = ((bf16[128,8,1024]{2,1,0:T(8,128)(2,1)}), bf16[128,8,1024]{2,1,0:T(8,128)(2,1)S(1)}, u32[]{:S(2)}, u32[]{:S(2)}) async-start(bf16[128,8,1024]{2,1,0:T(8,128)(2,1)} %bitcast.29), calls=%async_computation.1 | async-start | bytes 4194304 | tf_op jit(solution)/shard_map/all_to_all | solution.py:409
  59.2 5.8 %shared.1.base = f32[128,2048]{1,0:T(8,128)S(1)} custom-call(bf16[128,2048]{1,0:T(8,128)(2,1)} %get-tuple-element.19.normed, bf16[128,2048]{1,0:T(8,128)(2,1)} %get-tuple-element.20.stream, bf16[2048,512]{1,0:T(8,128)(2,1)} %gate.7, bf16[2048,512]{1,0:T(8,128)(2,1)} %up.1, bf16[512,2048]{1,0:T(8,128)(2,1)} %down.1), custom_call_target="tpu_custom_call" | custom-call | flops 8000000000 | bytes 1000 | tf_op jit(solution)/shard_map/shared/pallas_call | solution.py:270
  64.9 24.8 %all-to-all-done.1 = bf16[128,8,1024]{2,1,0:T(8,128)(2,1)S(1)} async-done(((bf16[128,8,1024]{2,1,0:T(8,128)(2,1)}), bf16[128,8,1024]{2,1,0:T(8,128)(2,1)S(1)}, u32[]{:S(2)}, u32[]{:S(2)}) %all-to-all-start.1) | async-done | bytes 2097184 | tf_op jit(solution)/shard_map/all_to_all | solution.py:409
  89.8 1.6 %gather.1 = bf16[128,2048]{1,0:T(8,128)(2,1)} custom-call(bf16[1024,1024]{1,0:T(8,128)(2,1)S(1)} %bitcast.13, f32[8,128]{1,0:T(8,128)S(1)} %get-tuple-element.18.meta, f32[128,2048]{1,0:T(8,128)S(1)} %shared.1.base), custom_call_target="tpu_custom_call" | custom-call | flops 2000000000 | bytes 1000 | tf_op jit(solution)/shard_map/gather/pallas_call | solution.py:270
Async XLA Ops:
  0.0 3.0 %copy-start.8 = (bf16[256,512]{1,0:T(8,128)(2,1)S(1)}, bf16[256,512]{1,0:T(8,128)(2,1)}, u32[]{:S(2)}) copy-start(bf16[256,512]{1,0:T(8,128)(2,1)} %gate.6) | copy-start | bytes 786436
  0.0 3.0 %copy-start.7 = (bf16[256,512]{1,0:T(8,128)(2,1)S(1)}, bf16[256,512]{1,0:T(8,128)(2,1)}, u32[]{:S(2)}) copy-start(bf16[256,512]{1,0:T(8,128)(2,1)} %value.5) | copy-start | bytes 786436
  0.0 3.0 %copy-start.13 = (s32[256]{0:T(256)S(1)}, s32[256]{0:T(256)}, u32[]{:S(2)}) copy-start(s32[256]{0:T(256)} %param.20) | copy-start | bytes 3076
  0.0 3.0 %copy-start.9 = (bf16[31,512]{1,0:T(8,128)(2,1)S(1)}, bf16[31,512]{1,0:T(8,128)(2,1)}, u32[]{:S(2)}) copy-start(bf16[31,512]{1,0:T(8,128)(2,1)} %taps.3) | copy-start | bytes 95236
  0.0 3.0 %copy-start.12 = (f32[512]{0:T(512)S(1)}, f32[512]{0:T(512)}, u32[]{:S(2)}) copy-start(f32[512]{0:T(512)} %param.22) | copy-start | bytes 6148
  0.0 3.0 %copy-start.11 = (f32[512]{0:T(512)S(1)}, f32[512]{0:T(512)}, u32[]{:S(2)}) copy-start(f32[512]{0:T(512)} %param.21) | copy-start | bytes 6148
  0.9 10.6 %collective-permute-start = (bf16[32,512]{1,0:T(8,128)(2,1)S(1)}, bf16[32,512]{1,0:T(8,128)(2,1)S(1)}, u32[]{:S(2)}, u32[]{:S(2)}) collective-permute-start(bf16[32,512]{1,0:T(8,128)(2,1)S(1)} %pack.1), channel_id=1, source_target_pairs={{0,2},{2,4},{4,6},{6,8},{8,10},{10,12},{12,14},{14,16},{16,18},{18... | collective-permute-start | bytes 98312 | tf_op jit(solution)/shard_map/ppermute | solution.py:20
  3.0 10.8 %copy-start = (bf16[1024,2048]{1,0:T(8,128)(2,1)S(1)}, bf16[1024,2048]{1,0:T(8,128)(2,1)}, u32[]{:S(2)}) copy-start(bf16[1024,2048]{1,0:T(8,128)(2,1)} %conv_out.3) | copy-start | bytes 12582916
  3.0 10.7 %copy-start.1 = (bf16[128,2048]{1,0:T(8,128)(2,1)S(1)}, bf16[128,2048]{1,0:T(8,128)(2,1)}, u32[]{:S(2)}) copy-start(bf16[128,2048]{1,0:T(8,128)(2,1)} %residual.1) | copy-start | bytes 1572868
  3.0 10.7 %copy-start.2 = (s32[128,2]{0,1:T(2,128)S(1)}, s32[128,2]{0,1:T(2,128)}, u32[]{:S(2)}) copy-start(s32[128,2]{0,1:T(2,128)} %param.26) | copy-start | bytes 3076
  3.1 10.7 %copy-start.3 = (f32[128,2]{0,1:T(2,128)S(1)}, f32[128,2]{0,1:T(2,128)}, u32[]{:S(2)}) copy-start(f32[128,2]{0,1:T(2,128)} %param.27) | copy-start | bytes 3076
  12.1 2.8 %collective-permute-start.1 = (bf16[128,512]{1,0:T(8,128)(2,1)S(1)}, bf16[128,512]{1,0:T(8,128)(2,1)S(1)}, u32[]{:S(2)}, u32[]{:S(2)}) collective-permute-start(bf16[128,512]{1,0:T(8,128)(2,1)S(1)} %get-tuple-element.13), channel_id=1, source_target_pairs={{0,1},{1,0},{2,3},{3,2},{4,5},{5,4},{6,7},{7,6},{8,9},{9,8},{10,11... | collective-permute-start | bytes 393224 | tf_op jit(solution)/shard_map/ppermute | solution.py:352
  13.8 1.1 %copy-start.10 = (f32[2048]{0:T(1024)S(1)}, f32[2048]{0:T(1024)}, u32[]{:S(2)}) copy-start(f32[2048]{0:T(1024)} %param.25) | copy-start | bytes 24580
  14.9 35.4 %copy-start.6 = (bf16[1,512,2048]{2,1,0:T(8,128)(2,1)S(1)}, bf16[1,512,2048]{2,1,0:T(8,128)(2,1)}, u32[]{:S(2)}) copy-start(bf16[1,512,2048]{2,1,0:T(8,128)(2,1)} %param.30) | copy-start | bytes 6291460
  16.5 33.9 %copy-start.4 = (bf16[1,2048,512]{2,1,0:T(8,128)(2,1)S(1)}, bf16[1,2048,512]{2,1,0:T(8,128)(2,1)}, u32[]{:S(2)}) copy-start(bf16[1,2048,512]{2,1,0:T(8,128)(2,1)} %param.28) | copy-start | bytes 6291460
  16.5 33.9 %copy-start.5 = (bf16[1,2048,512]{2,1,0:T(8,128)(2,1)S(1)}, bf16[1,2048,512]{2,1,0:T(8,128)(2,1)}, u32[]{:S(2)}) copy-start(bf16[1,2048,512]{2,1,0:T(8,128)(2,1)} %param.29) | copy-start | bytes 6291460
  54.8 35.0 %all-to-all-start.1 = ((bf16[128,8,1024]{2,1,0:T(8,128)(2,1)}), bf16[128,8,1024]{2,1,0:T(8,128)(2,1)S(1)}, u32[]{:S(2)}, u32[]{:S(2)}) async-start(bf16[128,8,1024]{2,1,0:T(8,128)(2,1)} %bitcast.29), calls=%async_computation.1 | async-start | bytes 4194304 | tf_op jit(solution)/shard_map/all_to_all | solution.py:409
